TPU v7x, 32 devices: a whole 2x2x4 slice. The times are simulated.
32 devices in a mesh: sp: 16 (over z, y, core), tp: 2 (over x).
Axes of the slice: x: 2, y: 2, z: 4, core: 2. Of those that a mesh axis runs over, the one named last changes fastest.
Arguments:
- asking_matrix: bfloat16 [2048, 2048], P('sp', 'tp'), may hold values from -30 to 30
- matching_key_matrix: bfloat16 [2048, 1024], P('sp', 'tp'), may hold values from -30 to 30
- carried_value_matrix: bfloat16 [2048, 1024], P('sp', 'tp'), may hold values from -48 to 48
- silu_switch_argument: bfloat16 [2048, 2048], P('sp', 'tp'), may hold values from -6 to 6
- duality_source_matrix: bfloat16 [2048, 2048], P('sp', 'tp'), may hold values from -6 to 6
- storing_direction_matrix: bfloat16 [2048, 1024], P('sp', 'tp'), may hold values from -6 to 6
- fetching_direction_matrix: bfloat16 [2048, 1024], P('sp', 'tp'), may hold values from -6 to 6
- duality_kernel_coefficients: bfloat16 [5, 2048], P(None, 'tp'), may hold values from -2.5 to 2.5
- storing_kernel_coefficients: bfloat16 [5, 1024], P(None, 'tp'), may hold values from -2.5 to 2.5
- fetching_kernel_coefficients: bfloat16 [5, 1024], P(None, 'tp'), may hold values from -2.5 to 2.5
- raw_increment_lengths: float32 [2, 32, 2048], P(None, 'tp', 'sp'), may hold values from -5.5 to 5.5
- logarithmic_fading_speeds: float32 [2, 32], P(None, 'tp'), may hold values from -16 to -2.9
- token_fading_spikes: float32 [2, 32, 2048], P(None, 'tp', 'sp'), may hold values from -2.1 to 0
- absorber_score_vector: float32 [16], P('tp'), may hold values from 4 to 8
- cluster_scaling_factor: float32 [2048], P('tp'), may hold values from 0.1 to 1.9
- final_mapping_matrix: bfloat16 [2, 2048, 4096], P(None, 'tp', 'sp'), may hold values from -0.09375 to 0.09375
Outputs:
- mixed_out: bfloat16 [2048, 4096], P(('sp', 'tp'))
All inputs are finite; a program needn't handle non-finite values.
Results may differ from a plain program's by a relative error of at most 0.014.
Values may be sent and summed in bfloat16 or wider, within the bound.
A program may use at most 128 MiB of HBM per device.

v0:
```python
import jax
import jax.numpy as jnp
from jax import lax
from jax.sharding import PartitionSpec as P

HEAD = 128
SSD_HEAD = 64
STATE = 128
CONV = 5
WINDOW = 128
SPAN = 128


ROTARY_BASE = 500000.0
EPSILON = 1e-06


def padded_2(cells, sides, width):
    for axis, dim in sides:
        count = lax.axis_size(axis)
        ends = count - 1
        head = lax.slice_in_dim(cells, 0, width, axis=dim)
        tail = lax.slice_in_dim(cells, cells.shape[dim] - width, cells.shape[dim], axis=dim)
        cells = jnp.concatenate(
            [
                lax.ppermute(tail, axis, [(i, (i + 1) % count) for i in range(ends)]),
                cells,
                lax.ppermute(head, axis, [((i + 1) % count, i) for i in range(ends)]),
            ],
            axis=dim,
        )
    return cells


def entering_2(part, axis, combine, identity, reverse):
    count = lax.axis_size(axis)
    place = lax.axis_index(axis)
    ahead = count - 1 - place if reverse else place
    gathered = jax.tree.map(lambda a: lax.all_gather(a, axis), part)
    state = jax.tree.map(lambda a, e: jnp.zeros_like(a) + jnp.asarray(e, a.dtype), part, identity)

    def one(turn, state):
        source = count - 1 - turn if reverse else turn
        return combine(
            state, jax.tree.map(lambda a: lax.dynamic_index_in_dim(a, source, 0, False), gathered)
        )

    return lax.fori_loop(0, ahead, one, state)


def rotate(matrix, offset):
    row_count = matrix.shape[0]
    halfway = HEAD // 2
    heads_here = matrix.shape[1] // HEAD
    spacing = ROTARY_BASE ** (-jnp.arange(halfway, dtype=jnp.float32) * 2.0 / HEAD)
    places = (offset + jnp.arange(row_count, dtype=jnp.int32)).astype(jnp.float32)
    angles = places[:, None] * spacing[None, :]
    cosine = jnp.cos(angles)[:, None, :]
    sine_table = jnp.sin(angles)[:, None, :]
    halves = matrix.astype(jnp.float32).reshape(row_count, heads_here, 2, halfway)
    former = halves[:, :, 0]
    latter = halves[:, :, 1]
    turned = jnp.stack(
        [former * cosine - latter * sine_table, latter * cosine + former * sine_table], axis=2
    )
    return turned.reshape(row_count, heads_here * HEAD).astype(jnp.bfloat16)


def banded(matrix, block_count, kv_here):
    stacked = matrix.reshape(block_count + 2, SPAN, kv_here, HEAD)
    return jnp.concatenate([stacked[:-2], stacked[1:-1], stacked[2:]], axis=1)


def attend(turned_queries, key_band, value_band, absorber_score_vector, offset, seq_total):
    row_count = turned_queries.shape[0]
    block_count = row_count // SPAN
    kv_here = key_band.shape[1] // HEAD
    sharing = turned_queries.shape[1] // HEAD // kv_here
    key_tiles = banded(key_band, block_count, kv_here)
    value_tiles = banded(value_band, block_count, kv_here)
    query_tiles = turned_queries.reshape(block_count, SPAN, kv_here, sharing, HEAD)
    scores = jnp.einsum(
        "bqkgd,bskd->bkgqs", query_tiles, key_tiles, preferred_element_type=jnp.float32
    ) * HEAD ** (-0.5)
    within = jnp.arange(SPAN, dtype=jnp.int32)[:, None]
    across = jnp.arange(3 * SPAN, dtype=jnp.int32)[None, :]
    inside = jnp.abs(across - SPAN - within) <= WINDOW
    places = offset - SPAN + jnp.arange(block_count, dtype=jnp.int32)[:, None] * SPAN + across
    present = (places >= 0) & (places < seq_total)
    allowed = inside[None, :, :] & present[:, None, :]
    scores = jnp.where(allowed[:, None, None, :, :], scores, -jnp.inf)
    sink_rows = absorber_score_vector.reshape(kv_here, sharing)[None, :, :, None, None]
    ceiling = jnp.maximum(jnp.max(scores, axis=-1, keepdims=True), sink_rows)
    weights = jnp.exp(scores - ceiling)
    denominator = jnp.sum(weights, axis=-1, keepdims=True) + jnp.exp(sink_rows - ceiling)
    probabilities = (weights / denominator).astype(jnp.bfloat16)
    attended = jnp.einsum(
        "bkgqs,bskd->bqkgd", probabilities, value_tiles, preferred_element_type=jnp.float32
    )
    return attended.reshape(row_count, turned_queries.shape[1]).astype(jnp.bfloat16)


def convolve(padded, taps_all, row_count):
    summed = jnp.zeros((row_count, padded.shape[1]), jnp.float32)
    for tap_index in range(CONV):
        summed = summed + padded[tap_index : tap_index + row_count].astype(jnp.float32) * taps_all[
            tap_index
        ].astype(jnp.float32)
    return jax.nn.silu(summed).astype(jnp.bfloat16)


def prepare(scan_rows, step_rows, decay_rows, write_rows, read_rows):
    row_count = scan_rows.shape[0]
    block_count = row_count // SPAN
    groups_here = write_rows.shape[1]
    per_group = scan_rows.shape[2]
    highest = lax.Precision.HIGHEST
    step_tiles = step_rows.reshape(block_count, SPAN, groups_here, per_group)
    scaled = (
        scan_rows.astype(jnp.float32).reshape(block_count, SPAN, groups_here, per_group, SSD_HEAD)
        * step_tiles[..., None]
    )
    running = jnp.cumsum(decay_rows.reshape(block_count, SPAN, groups_here, per_group), axis=1)
    write_tiles = write_rows.reshape(block_count, SPAN, groups_here, STATE)
    read_tiles = read_rows.reshape(block_count, SPAN, groups_here, STATE)
    earlier_mask = jnp.arange(SPAN)[:, None] >= jnp.arange(SPAN)[None, :]
    spread = running[:, :, None] - running[:, None, :]
    fading = jnp.exp(jnp.where(earlier_mask[None, :, :, None, None], spread, -jnp.inf))
    affinity = jnp.einsum(
        "blgn,bsgn->blsg", read_tiles, write_tiles, preferred_element_type=jnp.float32
    )
    within_block = jnp.einsum(
        "blsgr,bsgrp->blgrp", affinity[..., None] * fading, scaled, precision=highest
    )
    to_end = jnp.exp(running[:, -1:] - running)
    block_states = jnp.einsum(
        "blgn,blgrp->bgrpn",
        write_tiles.astype(jnp.float32),
        scaled * to_end[..., None],
        precision=highest,
    )
    totals = running[:, -1]

    def advance(carried, block_item):
        fresh_state, block_total = block_item
        return (carried * jnp.exp(block_total)[..., None, None] + fresh_state, carried)

    final_state, entering = lax.scan(
        advance, jnp.zeros(block_states.shape[1:], jnp.float32), (block_states, totals)
    )
    summary = (jnp.exp(jnp.sum(totals, axis=0)), final_state)
    return ((within_block, entering, running, totals, read_tiles), summary)


def finish(pieces, incoming):
    within_block, entering, running, totals, read_tiles = pieces
    before = jnp.cumsum(totals, axis=0) - totals
    starting = entering + incoming[None] * jnp.exp(before)[..., None, None]
    carried = (
        jnp.einsum(
            "blgn,bgrpn->blgrp",
            read_tiles.astype(jnp.float32),
            starting,
            precision=lax.Precision.HIGHEST,
        )
        * jnp.exp(running)[..., None]
    )
    joined = within_block + carried
    return joined.reshape(joined.shape[0] * SPAN, -1)


def linked(earlier, later):
    return (earlier[0] * later[0], earlier[1] * later[0][..., None, None] + later[1])


def local(
    asking_matrix,
    matching_key_matrix,
    carried_value_matrix,
    silu_switch_argument,
    duality_source_matrix,
    storing_direction_matrix,
    fetching_direction_matrix,
    duality_kernel_coefficients,
    storing_kernel_coefficients,
    fetching_kernel_coefficients,
    raw_increment_lengths,
    logarithmic_fading_speeds,
    token_fading_spikes,
    absorber_score_vector,
    cluster_scaling_factor,
    final_mapping_matrix,
):
    row_count = asking_matrix.shape[0]
    offset = lax.axis_index("sp") * row_count
    seq_total = lax.axis_size("sp") * row_count
    turned_queries = rotate(asking_matrix, offset)
    key_value = jnp.concatenate([rotate(matching_key_matrix, offset), carried_value_matrix], axis=1)
    raw_rows = jnp.concatenate(
        [duality_source_matrix, storing_direction_matrix, fetching_direction_matrix], axis=1
    )
    margin = CONV // 2
    pair_rims = padded_2(key_value, (("sp", 0),), WINDOW)
    raw_rims = padded_2(raw_rows, (("sp", 0),), margin)
    filler = jnp.zeros((SPAN - WINDOW, key_value.shape[1]), jnp.bfloat16)
    pair_band = jnp.concatenate([filler, pair_rims, filler], axis=0)
    kv_width = matching_key_matrix.shape[1]
    attended = attend(
        turned_queries,
        pair_band[:, :kv_width],
        pair_band[:, kv_width:],
        absorber_score_vector,
        offset,
        seq_total,
    )
    conved = convolve(
        raw_rims,
        jnp.concatenate(
            [
                duality_kernel_coefficients,
                storing_kernel_coefficients,
                fetching_kernel_coefficients,
            ],
            axis=1,
        ),
        row_count,
    )
    scan_width = duality_source_matrix.shape[1]
    write_width = storing_direction_matrix.shape[1]
    groups_here = write_width // STATE
    per_group = scan_width // SSD_HEAD // groups_here
    scan_rows = conved[:, :scan_width].reshape(row_count, groups_here, per_group, SSD_HEAD)
    write_rows = conved[:, scan_width : scan_width + write_width].reshape(
        row_count, groups_here, STATE
    )
    read_rows = conved[:, scan_width + write_width :].reshape(row_count, groups_here, STATE)
    joint_increment_lengths = jax.nn.softplus(raw_increment_lengths)
    joint_fading_amounts = (
        -jnp.exp(logarithmic_fading_speeds)[:, :, None] * joint_increment_lengths
        + token_fading_spikes
    )
    steps_rows = jnp.transpose(joint_increment_lengths, (0, 2, 1)).reshape(
        2, row_count, groups_here, per_group
    )
    decay_rows = jnp.transpose(joint_fading_amounts, (0, 2, 1)).reshape(
        2, row_count, groups_here, per_group
    )
    ahead_pieces, ahead_summary = prepare(
        scan_rows, steps_rows[0], decay_rows[0], write_rows, read_rows
    )
    back_pieces, back_summary = prepare(
        scan_rows[::-1], steps_rows[1][::-1], decay_rows[1][::-1], write_rows[::-1], read_rows[::-1]
    )
    identity = (
        jnp.ones((groups_here, per_group), jnp.float32),
        jnp.zeros((groups_here, per_group, SSD_HEAD, STATE), jnp.float32),
    )
    ahead_in = entering_2(ahead_summary, "sp", linked, identity, False)
    back_in = entering_2(back_summary, "sp", linked, identity, True)
    both_ways = finish(ahead_pieces, ahead_in[1]) + finish(back_pieces, back_in[1])[::-1]
    gated_rows = both_ways * jax.nn.silu(silu_switch_argument.astype(jnp.float32))
    grouped = gated_rows.reshape(row_count, groups_here, -1)
    grouped = grouped * lax.rsqrt(jnp.mean(grouped * grouped, axis=-1, keepdims=True) + EPSILON)
    normed = (grouped.reshape(row_count, scan_width) * cluster_scaling_factor).astype(jnp.bfloat16)
    mixed_rows = jnp.concatenate([attended, normed], axis=1)
    whole_weight = lax.all_gather(final_mapping_matrix, "sp", axis=2, tiled=True)
    stacked = whole_weight.reshape(-1, whole_weight.shape[2])
    return lax.psum_scatter(
        jnp.dot(mixed_rows, stacked, preferred_element_type=jnp.float32).astype(jnp.bfloat16),
        "tp",
        scatter_dimension=0,
        tiled=True,
    )


def solution(mesh):
    in_specs = (
        P("sp", "tp"),
        P("sp", "tp"),
        P("sp", "tp"),
        P("sp", "tp"),
        P("sp", "tp"),
        P("sp", "tp"),
        P("sp", "tp"),
        P(None, "tp"),
        P(None, "tp"),
        P(None, "tp"),
        P(None, "tp", "sp"),
        P(None, "tp"),
        P(None, "tp", "sp"),
        P("tp"),
        P("tp"),
        P(None, "tp", "sp"),
    )
    out_specs = P(("sp", "tp"), None)
    return jax.shard_map(local, mesh=mesh, in_specs=in_specs, out_specs=out_specs, check_vma=False)
```

profile of v0, /device:TPU:0, one launch (start us, length us, event | category | flops | bytes accessed | tf_op | source)
XLA Modules:
  0.0 351.5 jit_solution(15018297728650527483)
XLA Ops:
  6.6 1.1 copy.158
  7.8 1.0 copy.159
  8.8 1.0 copy.160
  10.1 2.4 collective-permute-start.2
  12.5 1.3 collective-permute-start.3
  14.0 0.6 fusion.70
  15.0 0.6 slice_bitcast_fusion
  15.8 0.6 subtract_exponential_fusion.3
  16.6 1.8 collective-permute-done.3
  18.4 0.7 maximum_maximum_fusion
  19.1 4.5 %multiply_convert_fusion = bf16[128,2048]{0,1:T(8,128)(2,1)S(1)} fusion(bf16[130,2048]{0,1:T(8,128)(2,1)S(1)} %get-tuple-element.190, bf16[130,2048]{0,1:T(8,128)(2,1)S(1)} %get-tuple-element.189, f32[2048]{0:T(1024)S(1)} %bitcast.195, f32[2048]{0:T(1024)S(1)} %bitcast.196, f32[2048]{0:T(1024)S(1)} %bitcast.197, f32[2048]{0:T(1024)S(1)} %bitcast.198, ...), kind=kLoop, calls=%fused_computation.32 | loop fusion | flops 6291456 | bytes 3186688 | tf_op jit(solution)/shard_map/convert_element_type | solution.py:109
  24.2 1.2 convolution_add_fusion
  26.2 1.2 convolution_add_fusion.1
  27.5 0.7 all-gather.8.cloned.1.call-update
  28.9 11.0 %collective-permute-start = (bf16[128,1024]{0,1:T(8,128)(2,1)S(1)}, bf16[128,1024]{0,1:T(8,128)(2,1)}, u32[]{:S(2)}, u32[]{:S(2)}) collective-permute-start(bf16[128,1024]{0,1:T(8,128)(2,1)S(1)} %pad_maximum_fusion.2), channel_id=1, source_target_pairs={{0,2},{2,4},{4,6},{6,8},{8,10},{10,12},{12,14},{14,16},{16,18},{18... | collective-permute-start | bytes 786440 | tf_op jit(solution)/shard_map/ppermute | solution.py:26
  39.9 1.3 collective-permute-start.1
  41.2 0.8 copy.153
  42.4 0.7 copy.175
  43.3 24.6 %all-gather.2 = f32[16,1,4,4]{3,2,1,0:T(4,128)S(1)} all-gather(f32[1,1,4,4]{3,2,1,0:T(4,128)S(1)} %copy-done.13), channel_id=4, replica_groups=mesh['sp'=16,'tp'=2] {'sp'}, dimensions={0}, use_global_device_ids=true | all-gather | bytes 1088 | tf_op jit(solution)/shard_map/all_gather | solution.py:39
  68.0 18.2 %all-gather = f32[16,1,4,4]{3,2,1,0:T(4,128)S(1)} all-gather(f32[1,1,4,4]{3,2,1,0:T(4,128)S(1)} %get-tuple-element.210), channel_id=2, replica_groups=mesh['sp'=16,'tp'=2] {'sp'}, dimensions={0}, use_global_device_ids=true | all-gather | bytes 1088 | tf_op jit(solution)/shard_map/all_gather | solution.py:39
  87.7 1.0 fusion.68
  88.8 1.0 fusion.69
  90.7 0.4 convolution_convert_fusion.1
  91.3 20.1 %all-gather.12.cloned.1.call-done = f32[64,4,64,128]{3,2,1,0:T(8,128)} async-done(((f32[4,4,64,128]{3,2,1,0:T(8,128)}), f32[64,4,64,128]{3,2,1,0:T(8,128)}) %all-gather.12.cloned.1.call-update) | async-done | bytes 8388624 | tf_op jit(solution)/shard_map/all_gather | solution.py:39
  111.5 18.6 %while.17 = (s32[]{:T(128)}, f32[4,4,64,128]{3,2,1,0:T(8,128)S(1)}, s32[]{:T(128)}, f32[16,4,4]{2,1,0:T(4,128)S(1)}, f32[16,4,4,64,128]{4,3,2,1,0:T(8,128)}, /*index=5*/s32[]{:T(128)}, s32[]{:T(128)}, s32[]{:T(128)}, s32[]{:T(128)}) while((s32[]{:T(128)}, f32[4,4,64,128]{3,2,1,0:T(8,128)S(1)}, s32[]{:T(128)}, f32[16,4,4]{2,1,0:T(4,128)S(1)}, ...), condition=%wide.region_7.8_spmd, body=%wide.region_6.7_spmd.sunk | while | flops 262150 | bytes 1573203 | solution.py:48
  111.5 1.2 bitcast_add_fusion.5
  112.8 1.2 bitcast_add_fusion.5
  114.0 1.2 bitcast_add_fusion.5
  115.2 1.2 bitcast_add_fusion.5
  116.5 1.2 bitcast_add_fusion.5
  117.7 1.2 bitcast_add_fusion.5
  118.9 1.2 bitcast_add_fusion.5
  120.2 1.2 bitcast_add_fusion.5
  121.5 1.2 bitcast_add_fusion.5
  122.7 1.2 bitcast_add_fusion.5
  123.9 1.2 bitcast_add_fusion.5
  125.2 1.2 bitcast_add_fusion.5
  126.4 1.2 bitcast_add_fusion.5
  127.6 1.2 bitcast_add_fusion.5
  128.9 1.2 bitcast_add_fusion.5
  130.1 0.4 fusion.4
  130.6 2.2 fusion.1
  133.2 53.3 %all-gather.10.cloned.1.call-done = f32[64,4,64,128]{3,2,1,0:T(8,128)} async-done(((f32[4,4,64,128]{3,2,1,0:T(8,128)}), f32[64,4,64,128]{3,2,1,0:T(8,128)}) %all-gather.10.cloned.1.call-update) | async-done | bytes 8388624 | tf_op jit(solution)/shard_map/all_gather | solution.py:39
  186.8 0.4 fusion.3
  187.2 2.2 fusion.2
  190.9 126.3 %all-gather.8.cloned.1.call-done = bf16[2,1024,4096]{2,1,0:T(8,128)(2,1)} async-done(((bf16[2,1024,256]{2,1,0:T(8,128)(2,1)}), bf16[2,1024,4096]{2,1,0:T(8,128)(2,1)}) %all-gather.8.cloned.1.call-update) | async-done | bytes 16777232 | tf_op jit(solution)/shard_map/all_gather | solution.py:266
  317.2 9.1 %convolution_convert_fusion = bf16[128,4096]{1,0:T(8,128)(2,1)} fusion(bf16[2048,4096]{1,0:T(8,128)(2,1)} %bitcast.163, bf16[128,1024]{1,0:T(8,128)(2,1)S(1)} %multiply_convert_fusion.1, bf16[128,1024]{1,0:T(8,128)(2,1)S(1)} %copy.185), kind=kOutput, calls=%fused_computation.4 | convolution fusion | flops 2149056512 | bytes 18350080 | tf_op jit(solution)/shard_map/dot_general | solution.py:269
  326.3 18.7 %reduce-scatter.2.cloned.1.call-done = bf16[64,4096]{1,0:T(8,128)(2,1)} async-done(((bf16[128,4096]{1,0:T(8,128)(2,1)}), bf16[64,4096]{1,0:T(8,128)(2,1)}) %reduce-scatter.2.cloned.1.call-update) | async-done | bytes 524304 | tf_op jit(solution)/shard_map/reduce_scatter | solution.py:268
  (133 shorter events, 8.5 us)
Async XLA Ops:
  6.5 7.3 %copy-start.7 = (bf16[5,1024]{1,0:T(8,128)(2,1)S(1)}, bf16[5,1024]{1,0:T(8,128)(2,1)}, u32[]{:S(2)}) copy-start(bf16[5,1024]{1,0:T(8,128)(2,1)} %param.27) | copy-start | bytes 30724
  6.5 7.3 %copy-start.14 = (bf16[5,512]{1,0:T(8,128)(2,1)S(1)}, bf16[5,512]{1,0:T(8,128)(2,1)}, u32[]{:S(2)}) copy-start(bf16[5,512]{1,0:T(8,128)(2,1)} %param.28) | copy-start | bytes 15364
  6.5 7.3 %copy-start.15 = (bf16[5,512]{1,0:T(8,128)(2,1)S(1)}, bf16[5,512]{1,0:T(8,128)(2,1)}, u32[]{:S(2)}) copy-start(bf16[5,512]{1,0:T(8,128)(2,1)} %param.29) | copy-start | bytes 15364
  6.5 7.4 %copy-start.17 = (f32[2,16]{1,0:T(2,128)S(1)}, f32[2,16]{1,0:T(2,128)}, u32[]{:S(2)}) copy-start(f32[2,16]{1,0:T(2,128)} %param.31) | copy-start | bytes 388
  6.5 7.4 %copy-start.8 = (f32[2,16,128]{2,1,0:T(8,128)S(1)}, f32[2,16,128]{2,1,0:T(8,128)}, u32[]{:S(2)}) copy-start(f32[2,16,128]{2,1,0:T(8,128)} %param.30) | copy-start | bytes 49156
  6.5 7.4 %copy-start.9 = (f32[2,16,128]{2,1,0:T(8,128)S(1)}, f32[2,16,128]{2,1,0:T(8,128)}, u32[]{:S(2)}) copy-start(f32[2,16,128]{2,1,0:T(8,128)} %param.32) | copy-start | bytes 49156
  6.6 104.9 %all-gather.12.cloned.1.call-start = ((), (), s32[]{:S(2)}) async-start(), calls=%async_computation.4 | async-start | bytes 8912896 | tf_op jit(solution)/shard_map/all_gather | solution.py:39
  10.1 6.5 %collective-permute-start.2 = (bf16[2,2048]{0,1:T(8,128)(2,1)S(1)}, bf16[2,2048]{0,1:T(8,128)(2,1)S(1)}, u32[]{:S(2)}, u32[]{:S(2)}) collective-permute-start(bf16[2,2048]{0,1:T(8,128)(2,1)S(1)} %get-tuple-element.191), channel_id=1, source_target_pairs={{0,2},{2,4},{4,6},{6,8},{8,10},{10,12},{12,14},{14,16},{16,18},{18... | collective-permute-start | bytes 24584 | tf_op jit(solution)/shard_map/ppermute | solution.py:26
  12.5 5.9 %collective-permute-start.3 = (bf16[2,2048]{0,1:T(8,128)(2,1)S(1)}, bf16[2,2048]{0,1:T(8,128)(2,1)S(1)}, u32[]{:S(2)}, u32[]{:S(2)}) collective-permute-start(bf16[2,2048]{0,1:T(8,128)(2,1)S(1)} %get-tuple-element.192), channel_id=1, source_target_pairs={{2,0},{4,2},{6,4},{8,6},{10,8},{12,10},{14,12},{16,14},{18,16},{20... | collective-permute-start | bytes 24584 | tf_op jit(solution)/shard_map/ppermute | solution.py:28
  19.1 5.2 %copy-start.11 = (f32[4,4]{1,0:T(4,128)S(1)}, f32[4,4]{1,0:T(4,128)}, u32[]{:S(2)}) copy-start(f32[4,4]{1,0:T(4,128)} %get-tuple-element.200) | copy-start | bytes 196
  23.6 2.0 copy-start.6
  23.6 2.5 copy-start.5
  25.5 161.0 %all-gather.10.cloned.1.call-start = ((), (), s32[]{:S(2)}) async-start(), calls=%async_computation.3 | async-start | bytes 8912896 | tf_op jit(solution)/shard_map/all_gather | solution.py:39
  25.7 2.5 copy-start.2
  25.9 2.5 copy-start.3
  27.4 14.5 %copy-start.1 = (bf16[128,1024]{1,0:T(8,128)(2,1)S(1)}, bf16[128,1024]{1,0:T(8,128)(2,1)}, u32[]{:S(2)}) copy-start(bf16[128,1024]{1,0:T(8,128)(2,1)} %param.20) | copy-start | bytes 786436
  27.4 289.8 %all-gather.8.cloned.1.call-start = ((), (), s32[]{:S(2)}) async-start(), calls=%async_computation.1 | async-start | bytes 17825792 | tf_op jit(solution)/shard_map/all_gather | solution.py:266
  28.2 14.0 %copy-start.18 = (f32[8]{0:T(128)S(1)}, f32[8]{0:T(128)}, u32[]{:S(2)}) copy-start(f32[8]{0:T(128)} %param.33) | copy-start | bytes 100
  28.2 316.8 %reduce-scatter.2.cloned.1.call-start = ((), (), s32[]{:S(2)}) async-start(), calls=%async_computation.2 | async-start | bytes 1572864 | tf_op jit(solution)/shard_map/reduce_scatter | solution.py:268
  28.4 14.9 %copy-start.13 = (f32[1,1,4,4]{3,2,1,0:T(4,128)S(1)}, f32[1,1,4,4]{3,2,1,0:T(4,128)}, u32[]{:S(2)}) copy-start(f32[1,1,4,4]{3,2,1,0:T(4,128)} %get-tuple-element.204) | copy-start | bytes 196
  28.9 58.8 %collective-permute-start = (bf16[128,1024]{0,1:T(8,128)(2,1)S(1)}, bf16[128,1024]{0,1:T(8,128)(2,1)}, u32[]{:S(2)}, u32[]{:S(2)}) collective-permute-start(bf16[128,1024]{0,1:T(8,128)(2,1)S(1)} %pad_maximum_fusion.2), channel_id=1, source_target_pairs={{0,2},{2,4},{4,6},{6,8},{8,10},{10,12},{12,14},{14,16},{16,18},{18... | collective-permute-start | bytes 786440 | tf_op jit(solution)/shard_map/ppermute | solution.py:26
  39.9 48.9 %collective-permute-start.1 = (bf16[128,1024]{0,1:T(8,128)(2,1)S(1)}, bf16[128,1024]{0,1:T(8,128)(2,1)}, u32[]{:S(2)}, u32[]{:S(2)}) collective-permute-start(bf16[128,1024]{0,1:T(8,128)(2,1)S(1)} %pad_maximum_fusion.2), channel_id=1, source_target_pairs={{2,0},{4,2},{6,4},{8,6},{10,8},{12,10},{14,12},{16,14},{18,16},{20... | collective-permute-start | bytes 786440 | tf_op jit(solution)/shard_map/ppermute | solution.py:28
  86.4 3.6 %copy-start.4 = (bf16[1,128,4,128]{3,1,2,0:T(8,128)(2,1)S(1)}, bf16[1,128,4,128]{3,1,2,0:T(8,128)(2,1)}, u32[]{:S(2)}) copy-start(bf16[1,128,4,128]{3,1,2,0:T(8,128)(2,1)} %copy.153) | copy-start | bytes 393220
  111.5 18.6 %copy-start.10 = (f32[4,4]{1,0:T(4,128)S(1)}, f32[4,4]{1,0:T(4,128)}, u32[]{:S(2)}) copy-start(f32[4,4]{1,0:T(4,128)} %get-tuple-element.199) | copy-start | bytes 196
  111.5 19.1 %copy-start.12 = (f32[128,4,4]{0,2,1:T(4,128)S(1)}, f32[128,4,4]{0,2,1:T(4,128)}, u32[]{:S(2)}) copy-start(f32[128,4,4]{0,2,1:T(4,128)} %copy.175) | copy-start | bytes 24580
  186.8 2.9 copy-start
  189.9 0.8 copy-start.16
Sparse Core Ops, SparseCore 0:
  25.6 85.7 all-gather.11
  113.6 72.8 all-gather.9
  188.7 128.4 all-gather.7
  326.4 18.5 reduce-scatter.1
where the time goes:
time: 353 us; the launch traced here: 352 us
  waiting for transfers between devices  221 us (63%)
  blocking collectives  42.9 us (12%)
  other arithmetic  26 us (7%)
  matrix products  18.1 us (5%)
  starting transfers between devices  16.2 us (5%)
  between operations  13.9 us (4%)
  local copies, waits for them, and re-layouts  12.8 us (4%)
    all_gather x1, waiting for transfers between devices, local(): lax.all_gather(final_mapping_matrix, 'sp', axis=2, tiled=True)  126 us
    all_gather x2, waiting for transfers between devices, entering_2(): gathered = jax.tree.map(lambda a: lax.all_gather(a, axis), part)  73.4 us
    all_gather x2, blocking collectives, entering_2(): gathered = jax.tree.map(lambda a: lax.all_gather(a, axis), part)  42.9 us
    reduce_scatter x1, waiting for transfers between devices, local(): lax.psum_scatter(jnp.dot(mixed_rows, stacked, preferred_element_type=jnp....  18.7 us
    add x15, other arithmetic, linked(): earlier[1] * later[0][..., None, None] + later[1]  17.9 us
    ppermute x2, starting transfers between devices, padded_2(): lax.ppermute(tail, axis, [(i, (i + 1) % count) for i in range(ends)])  13.5 us
    dot_general x1, matrix products, local(): jnp.dot(mixed_rows, stacked, preferred_element_type=jnp.float32)  9.08 us
  transfers between devices with their start and end apart: 8, of which 5 were waited for; matrix products, arithmetic and copies ran while one was open for 11% of the time, Pallas kernels for 0%

commit v1 on v0

--- a/solution.py
+++ b/solution.py
@@ -1,6 +1,10 @@
+import functools
+
 import jax
 import jax.numpy as jnp
 from jax import lax
+from jax.experimental import pallas as pl
+from jax.experimental.pallas import tpu as pltpu
 from jax.sharding import PartitionSpec as P
 
 HEAD = 128
@@ -32,20 +36,370 @@
     return cells
 
 
-def entering_2(part, axis, combine, identity, reverse):
-    count = lax.axis_size(axis)
-    place = lax.axis_index(axis)
-    ahead = count - 1 - place if reverse else place
-    gathered = jax.tree.map(lambda a: lax.all_gather(a, axis), part)
-    state = jax.tree.map(lambda a, e: jnp.zeros_like(a) + jnp.asarray(e, a.dtype), part, identity)
-
-    def one(turn, state):
-        source = count - 1 - turn if reverse else turn
-        return combine(
-            state, jax.tree.map(lambda a: lax.dynamic_index_in_dim(a, source, 0, False), gathered)
-        )
-
-    return lax.fori_loop(0, ahead, one, state)
+def clique_of(count):
+    return 4 if count % 4 == 0 else (2 if count % 2 == 0 else 1)
+
+
+def greet(partners):
+    barrier = pltpu.get_barrier_semaphore()
+    for partner in partners:
+        pl.semaphore_signal(
+            barrier, inc=1, device_id=partner, device_id_type=pl.DeviceIdType.MESH
+        )
+    pl.semaphore_wait(barrier, len(partners))
+
+
+def sending(source, target, send_sem, recv_sem, partner):
+    return pltpu.make_async_remote_copy(
+        src_ref=source,
+        dst_ref=target,
+        send_sem=send_sem,
+        recv_sem=recv_sem,
+        device_id=partner,
+        device_id_type=pl.DeviceIdType.MESH,
+    )
+
+
+def scan_kernel(
+    clique,
+    outer,
+    state_ref,
+    decay_ref,
+    out_ref,
+    near,
+    near_decay,
+    prefix,
+    before,
+    whole,
+    whole_decay,
+    far,
+    far_decay,
+    carry,
+    replies,
+    near_sems,
+    far_sems,
+    reply_sems,
+):
+    me = lax.axis_index("sp")
+    spot = lax.rem(me, clique)
+    layer = me // clique
+    base = me - spot
+    mates = [lax.rem(spot + d, clique) for d in range(1, clique)]
+    layers = [lax.rem(layer + d, outer) for d in range(1, outer)]
+    greet(
+        [{"sp": base + mate} for mate in mates]
+        + [{"sp": other * clique + spot} for other in layers]
+    )
+
+    def near_copy(mate, slot, sem_slot):
+        who = {"sp": base + mate}
+        return (
+            sending(
+                state_ref.at[mate],
+                near.at[slot],
+                near_sems.at[0, mate],
+                near_sems.at[1, sem_slot],
+                who,
+            ),
+            sending(
+                decay_ref.at[mate],
+                near_decay.at[slot],
+                near_sems.at[2, mate],
+                near_sems.at[3, sem_slot],
+                who,
+            ),
+        )
+
+    for mate in mates:
+        for copy in near_copy(mate, spot, spot):
+            copy.start()
+    near[spot] = state_ref[spot]
+    near_decay[spot] = decay_ref[spot]
+    for mate in mates:
+        for copy in near_copy(mate, mate, mate):
+            copy.wait_recv()
+    for way in range(2):
+        order = range(clique) if way == 0 else range(clique - 1, -1, -1)
+        running = jnp.zeros(prefix.shape[2:], jnp.float32)
+        product = jnp.ones(before.shape[2:], jnp.float32)
+        for turn in order:
+            prefix[turn, way] = running
+            before[turn, way] = product
+            factor = near_decay[turn, way]
+            running = running * factor[:, None, :] + near[turn, way].astype(jnp.float32)
+            product = product * factor
+        whole[way] = running.astype(jnp.bfloat16)
+        whole_decay[way] = product
+
+    def far_copy(way, other, slot):
+        who = {"sp": other * clique + spot}
+        return (
+            sending(
+                whole.at[way],
+                far.at[way, slot],
+                far_sems.at[0, way, other],
+                far_sems.at[1, way, slot],
+                who,
+            ),
+            sending(
+                whole_decay.at[way],
+                far_decay.at[way, slot],
+                far_sems.at[2, way, other],
+                far_sems.at[3, way, slot],
+                who,
+            ),
+        )
+
+    def later(way, first, second):
+        return second > first if way == 0 else second < first
+
+    for other in layers:
+        for way in range(2):
+
+            @pl.when(later(way, layer, other))
+            def _():
+                for copy in far_copy(way, other, layer):
+                    copy.start()
+
+    carry[...] = jnp.zeros_like(carry)
+    for way in range(2):
+        order = range(outer) if way == 0 else range(outer - 1, -1, -1)
+        for other in order:
+
+            @pl.when(later(way, other, layer))
+            def _():
+                for copy in far_copy(way, other, other):
+                    copy.wait_recv()
+                carry[way] = carry[way] * far_decay[way, other][:, None, :] + far[
+                    way, other
+                ].astype(jnp.float32)
+
+    for turn in range(clique):
+        for way in range(2):
+            replies[turn, way] = (
+                prefix[turn, way] + carry[way] * before[turn, way][:, None, :]
+            ).astype(jnp.bfloat16)
+
+    def reply(mate, slot):
+        return sending(
+            replies.at[mate],
+            out_ref.at[slot],
+            reply_sems.at[0, mate],
+            reply_sems.at[1, slot],
+            {"sp": base + mate},
+        )
+
+    for mate in mates:
+        reply(mate, spot).start()
+    out_ref[spot] = replies[spot]
+    for mate in mates:
+        reply(mate, mate).wait_recv()
+    for mate in mates:
+        for copy in near_copy(mate, spot, spot):
+            copy.wait_send()
+        reply(mate, spot).wait_send()
+    for other in layers:
+        for way in range(2):
+
+            @pl.when(later(way, layer, other))
+            def _():
+                for copy in far_copy(way, other, layer):
+                    copy.wait_send()
+
+
+def scan_states(states, decays):
+    count = lax.axis_size("sp")
+    clique = clique_of(count)
+    outer = count // clique
+    ways, heads, rows, cols = states.shape
+    part = heads // clique
+    states = states.reshape(ways, clique, part, rows, cols).transpose(1, 0, 2, 3, 4)
+    decays = jnp.broadcast_to(
+        decays.reshape(ways, clique, part).transpose(1, 0, 2)[..., None],
+        (clique, ways, part, cols),
+    )
+    block = (part, rows, cols)
+    whole_out = pl.pallas_call(
+        functools.partial(scan_kernel, clique, outer),
+        out_shape=jax.ShapeDtypeStruct((clique, ways) + block, jnp.bfloat16),
+        in_specs=[pl.BlockSpec(memory_space=pltpu.VMEM)] * 2,
+        out_specs=pl.BlockSpec(memory_space=pltpu.VMEM),
+        scratch_shapes=[
+            pltpu.VMEM((clique, ways) + block, jnp.bfloat16),
+            pltpu.VMEM((clique, ways, part, cols), jnp.float32),
+            pltpu.VMEM((clique, ways) + block, jnp.float32),
+            pltpu.VMEM((clique, ways, part, cols), jnp.float32),
+            pltpu.VMEM((ways,) + block, jnp.bfloat16),
+            pltpu.VMEM((ways, part, cols), jnp.float32),
+            pltpu.VMEM((ways, outer) + block, jnp.bfloat16),
+            pltpu.VMEM((ways, outer, part, cols), jnp.float32),
+            pltpu.VMEM((ways,) + block, jnp.float32),
+            pltpu.VMEM((clique, ways) + block, jnp.bfloat16),
+            pltpu.SemaphoreType.DMA((4, clique)),
+            pltpu.SemaphoreType.DMA((4, 2, outer)),
+            pltpu.SemaphoreType.DMA((2, clique)),
+        ],
+        compiler_params=pltpu.CompilerParams(collective_id=1, has_side_effects=True),
+    )(states.astype(jnp.bfloat16), decays)
+    return whole_out.transpose(1, 0, 2, 3, 4).reshape(ways, heads, rows, cols)
+
+
+def project_kernel(
+    clique,
+    outer,
+    tps,
+    mixed_ref,
+    *rest,
+):
+    weight_refs = rest[:clique]
+    (
+        out_ref,
+        gathered,
+        partial,
+        pieces,
+        summed,
+        mixed_sems,
+        piece_sems,
+        out_sems,
+    ) = rest[clique:]
+    me = lax.axis_index("sp")
+    lane = lax.axis_index("tp")
+    spot = lax.rem(me, clique)
+    layer = me // clique
+    layers = [lax.rem(layer + d, outer) for d in range(1, outer)]
+    lanes = [lax.rem(lane + d, tps) for d in range(1, tps)]
+
+    def at_layer(other):
+        return {"sp": other * clique + spot}
+
+    greet([at_layer(other) for other in layers] + [{"tp": other} for other in lanes])
+    share = mixed_ref.shape[1] // tps
+
+    def mixed_copy(other, slot):
+        return sending(
+            mixed_ref,
+            gathered.at[slot],
+            mixed_sems.at[0, other],
+            mixed_sems.at[1, slot],
+            at_layer(other),
+        )
+
+    def piece_copy(block, other, slot):
+        return sending(
+            partial.at[block, other],
+            pieces.at[block, slot],
+            piece_sems.at[0, block, other],
+            piece_sems.at[1, block, slot],
+            {"tp": other},
+        )
+
+    def out_copy(other, slot):
+        return sending(
+            summed.at[other],
+            out_ref.at[slot],
+            out_sems.at[0, other],
+            out_sems.at[1, slot],
+            at_layer(other),
+        )
+
+    for other in layers:
+        mixed_copy(other, layer).start()
+    gathered[layer] = mixed_ref[...]
+    order = [layer] + [lax.rem(layer + outer - d, outer) for d in range(1, outer)]
+
+    def multiply(block):
+        for flip, weight_ref in enumerate(weight_refs):
+            column = flipped(spot, flip)
+            product = jnp.dot(
+                gathered[block, 0], weight_ref[0], preferred_element_type=jnp.float32
+            ) + jnp.dot(
+                gathered[block, 1], weight_ref[1], preferred_element_type=jnp.float32
+            )
+            rounded = product.astype(jnp.bfloat16)
+            for other in range(tps):
+                partial[block, other, column] = rounded[other * share : (other + 1) * share]
+        for other in lanes:
+            piece_copy(block, other, lane).start()
+
+    def settle(block, own):
+        total = partial[block, lane].astype(jnp.float32)
+        for other in lanes:
+            piece_copy(block, other, other).wait_recv()
+            total = total + pieces[block, other].astype(jnp.float32)
+        summed[block] = total.astype(jnp.bfloat16)
+        if own:
+            out_ref[layer] = summed[layer]
+        else:
+            out_copy(block, layer).start()
+
+    for turn, block in enumerate(order):
+        if turn:
+            mixed_copy(block, block).wait_recv()
+        multiply(block)
+        if turn:
+            settle(order[turn - 1], turn == 1)
+    settle(order[-1], outer == 1)
+    for other in layers:
+        out_copy(other, other).wait_recv()
+    for other in layers:
+        mixed_copy(other, layer).wait_send()
+        out_copy(other, layer).wait_send()
+    for block in order:
+        for other in lanes:
+            piece_copy(block, other, lane).wait_send()
+
+
+def clique_weights(weight):
+    count = lax.axis_size("sp")
+    clique = clique_of(count)
+    held = [weight]
+    steps = []
+    step = clique // 2
+    while step:
+        pairs = [(i, (i // clique) * clique + ((i % clique) ^ step)) for i in range(count)]
+        held = held + [lax.ppermute(block, "sp", pairs) for block in held]
+        steps = steps + [step] if steps else [step]
+        step //= 2
+    flips = [0]
+    for step in steps:
+        flips = flips + [flip ^ step for flip in flips]
+    return [block for _, block in sorted(zip(flips, held), key=lambda item: item[0])]
+
+
+def flipped(spot, flip):
+    bit = 1
+    while bit <= flip:
+        if flip & bit:
+            spot = spot + bit - 2 * bit * lax.rem(spot // bit, 2)
+        bit *= 2
+    return spot
+
+
+def project(mixed, weights):
+    count = lax.axis_size("sp")
+    tps = lax.axis_size("tp")
+    clique = clique_of(count)
+    outer = count // clique
+    rows = mixed.shape[1]
+    width = weights[0].shape[2]
+    share = rows // tps
+    out = pl.pallas_call(
+        functools.partial(project_kernel, clique, outer, tps),
+        out_shape=jax.ShapeDtypeStruct((outer, clique, share, width), jnp.bfloat16),
+        in_specs=[pl.BlockSpec(memory_space=pltpu.VMEM)] * (1 + clique),
+        out_specs=pl.BlockSpec(memory_space=pltpu.VMEM),
+        scratch_shapes=[
+            pltpu.VMEM((outer,) + mixed.shape, jnp.bfloat16),
+            pltpu.VMEM((outer, tps, clique, share, width), jnp.bfloat16),
+            pltpu.VMEM((outer, tps, clique, share, width), jnp.bfloat16),
+            pltpu.VMEM((outer, clique, share, width), jnp.bfloat16),
+            pltpu.SemaphoreType.DMA((2, outer)),
+            pltpu.SemaphoreType.DMA((2, outer, tps)),
+            pltpu.SemaphoreType.DMA((2, outer)),
+        ],
+        compiler_params=pltpu.CompilerParams(collective_id=2, has_side_effects=True),
+    )(mixed, *weights)
+    return out.transpose(2, 0, 1, 3).reshape(share, outer * clique * width)
 
 
 def rotate(matrix, offset):
@@ -114,7 +468,6 @@
     block_count = row_count // SPAN
     groups_here = write_rows.shape[1]
     per_group = scan_rows.shape[2]
-    highest = lax.Precision.HIGHEST
     step_tiles = step_rows.reshape(block_count, SPAN, groups_here, per_group)
     scaled = (
         scan_rows.astype(jnp.float32).reshape(block_count, SPAN, groups_here, per_group, SSD_HEAD)
@@ -130,14 +483,13 @@
         "blgn,bsgn->blsg", read_tiles, write_tiles, preferred_element_type=jnp.float32
     )
     within_block = jnp.einsum(
-        "blsgr,bsgrp->blgrp", affinity[..., None] * fading, scaled, precision=highest
+        "blsgr,bsgrp->blgrp", affinity[..., None] * fading, scaled
     )
     to_end = jnp.exp(running[:, -1:] - running)
     block_states = jnp.einsum(
         "blgn,blgrp->bgrpn",
         write_tiles.astype(jnp.float32),
         scaled * to_end[..., None],
-        precision=highest,
     )
     totals = running[:, -1]
 
@@ -161,16 +513,11 @@
             "blgn,bgrpn->blgrp",
             read_tiles.astype(jnp.float32),
             starting,
-            precision=lax.Precision.HIGHEST,
         )
         * jnp.exp(running)[..., None]
     )
     joined = within_block + carried
     return joined.reshape(joined.shape[0] * SPAN, -1)
-
-
-def linked(earlier, later):
-    return (earlier[0] * later[0], earlier[1] * later[0][..., None, None] + later[1])
 
 
 def local(
@@ -194,6 +541,7 @@
     row_count = asking_matrix.shape[0]
     offset = lax.axis_index("sp") * row_count
     seq_total = lax.axis_size("sp") * row_count
+    weights = clique_weights(final_mapping_matrix)
     turned_queries = rotate(asking_matrix, offset)
     key_value = jnp.concatenate([rotate(matching_key_matrix, offset), carried_value_matrix], axis=1)
     raw_rows = jnp.concatenate(
@@ -251,26 +599,19 @@
     back_pieces, back_summary = prepare(
         scan_rows[::-1], steps_rows[1][::-1], decay_rows[1][::-1], write_rows[::-1], read_rows[::-1]
     )
-    identity = (
-        jnp.ones((groups_here, per_group), jnp.float32),
-        jnp.zeros((groups_here, per_group, SSD_HEAD, STATE), jnp.float32),
-    )
-    ahead_in = entering_2(ahead_summary, "sp", linked, identity, False)
-    back_in = entering_2(back_summary, "sp", linked, identity, True)
-    both_ways = finish(ahead_pieces, ahead_in[1]) + finish(back_pieces, back_in[1])[::-1]
+    heads = groups_here * per_group
+    incoming = scan_states(
+        jnp.stack([ahead_summary[1], back_summary[1]]).reshape(2, heads, SSD_HEAD, STATE),
+        jnp.stack([ahead_summary[0], back_summary[0]]).reshape(2, heads),
+    ).reshape(2, groups_here, per_group, SSD_HEAD, STATE)
+    both_ways = finish(ahead_pieces, incoming[0].astype(jnp.float32)) + finish(
+        back_pieces, incoming[1].astype(jnp.float32)
+    )[::-1]
     gated_rows = both_ways * jax.nn.silu(silu_switch_argument.astype(jnp.float32))
     grouped = gated_rows.reshape(row_count, groups_here, -1)
     grouped = grouped * lax.rsqrt(jnp.mean(grouped * grouped, axis=-1, keepdims=True) + EPSILON)
     normed = (grouped.reshape(row_count, scan_width) * cluster_scaling_factor).astype(jnp.bfloat16)
-    mixed_rows = jnp.concatenate([attended, normed], axis=1)
-    whole_weight = lax.all_gather(final_mapping_matrix, "sp", axis=2, tiled=True)
-    stacked = whole_weight.reshape(-1, whole_weight.shape[2])
-    return lax.psum_scatter(
-        jnp.dot(mixed_rows, stacked, preferred_element_type=jnp.float32).astype(jnp.bfloat16),
-        "tp",
-        scatter_dimension=0,
-        tiled=True,
-    )
+    return project(jnp.stack([attended, normed]), weights)
 
 
 def solution(mesh):

time: 353 us -> 164 us (0.46)
  waiting for transfers between devices: 221 us -> 0.67 us
  Pallas kernels: 0 us -> 97.9 us
  blocking collectives: 42.9 us -> 0 us
  between operations: 13.9 us -> 0.88 us
  local copies, waits for them, and re-layouts: 12.8 us -> 24 us
  matrix products: 18.1 us -> 6.94 us
  other arithmetic: 26 us -> 16.1 us
    all_gather x3 -> x0, waiting for transfers between devices: 200 us -> none  [the longest x1 126 us: local(): lax.all_gather(final_mapping_matrix, 'sp', axis=2, tiled=True)]
    pallas_call x0 -> x2, Pallas kernels: none -> 97.9 us  [the longest x1 73.1 us: project(): pl.pallas_call(functools.partial(project_kernel, clique, outer, tps), out...]
    all_gather x2 -> x0, blocking collectives: 42.9 us -> none  [entering_2(): gathered = jax.tree.map(lambda a: lax.all_gather(a, axis), part)]
    reduce_scatter x1 -> x0, waiting for transfers between devices: 18.7 us -> none  [local(): lax.psum_scatter(jnp.dot(mixed_rows, stacked, preferred_element_type=jnp....]
    add x15 -> x0, other arithmetic: 17.9 us -> none  [linked(): earlier[1] * later[0][..., None, None] + later[1]]
    dot_general x5 -> x4, matrix products: 14.4 us -> 5.18 us  [the longest x2 3.68 us: prepare(): jnp.einsum('blsgr,bsgrp->blgrp', affinity[..., None] * fading, scaled)]
    ppermute x0 -> x3, starting transfers between devices: none -> 6.32 us  [clique_weights(): held = held + [lax.ppermute(block, 'sp', pairs) for block in held]]
    ppermute x2, starting transfers between devices: 13.5 us -> 8.5 us  [padded_2(): lax.ppermute(tail, axis, [(i, (i + 1) % count) for i in range(ends)])]
  transfers between devices with their start and end apart: 8 -> 7, of which waited for: 5 -> 1; matrix products, arithmetic and copies ran while one was open for 11% -> 25% of each run, Pallas kernels for 0% -> 15%
where the time goes in v1:
time: 164 us
  Pallas kernels  97.9 us (60%)
  local copies, waits for them, and re-layouts  24 us (15%)
  starting transfers between devices  17.4 us (11%)
  other arithmetic  16.1 us (10%)
  matrix products  6.94 us (4%)
    pallas_call x1, Pallas kernels, project(): pl.pallas_call(functools.partial(project_kernel, clique, outer, tps), out...  73.1 us
    pallas_call x1, Pallas kernels, scan_states(): pl.pallas_call(functools.partial(scan_kernel, clique, outer), out_shape=j...  24.9 us
    ppermute x2, starting transfers between devices, padded_2(): lax.ppermute(tail, axis, [(i, (i + 1) % count) for i in range(ends)])  8.5 us
    ppermute x3, starting transfers between devices, clique_weights(): held = held + [lax.ppermute(block, 'sp', pairs) for block in held]  6.32 us
    convert_element_type x1, other arithmetic, convolve(): return jax.nn.silu(summed).astype(jnp.bfloat16)  4.47 us
    unnamed x83, local copies, waits for them, and re-layouts  3.9 us
    dot_general x2, matrix products, prepare(): jnp.einsum('blsgr,bsgrp->blgrp', affinity[..., None] * fading, scaled)  3.68 us
  transfers between devices with their start and end apart: 7, of which 1 were waited for; matrix products, arithmetic and copies ran while one was open for 25% of the time, Pallas kernels for 15%

profile of v1, /device:TPU:0, one launch (start us, length us, event | category | flops | bytes accessed | tf_op | source)
XLA Modules:
  0.0 163.9 jit_solution(10280907031059370098)
XLA Ops:
  0.0 1.1 copy.119
  1.1 1.0 copy.120
  2.4 0.7 pad_maximum_fusion.3
  3.2 3.1 %collective-permute-start = (bf16[128,1024]{0,1:T(8,128)(2,1)}, bf16[128,1024]{0,1:T(8,128)(2,1)}, u32[]{:S(2)}, u32[]{:S(2)}) collective-permute-start(bf16[128,1024]{0,1:T(8,128)(2,1)} %pad_maximum_fusion.3), channel_id=1, source_target_pairs={{0,2},{2,4},{4,6},{6,8},{8,10},{10,12},{12,14},{14,16},{16,18},{18... | collective-permute-start | bytes 786440 | tf_op jit(solution)/shard_map/ppermute | solution.py:30
  6.3 1.3 collective-permute-start.1
  8.1 1.1 fusion.74
  9.3 5.4 %collective-permute-start.2 = (bf16[2,2048]{0,1:T(8,128)(2,1)}, bf16[2,2048]{0,1:T(8,128)(2,1)}, u32[]{:S(2)}, u32[]{:S(2)}) collective-permute-start(bf16[2,2048]{0,1:T(8,128)(2,1)} %get-tuple-element.34), channel_id=1, source_target_pairs={{0,2},{2,4},{4,6},{6,8},{8,10},{10,12},{12,14},{14,16},{16,18},{18... | collective-permute-start | bytes 24584 | tf_op jit(solution)/shard_map/ppermute | solution.py:30
  14.6 1.3 collective-permute-start.3
  15.9 3.3 %collective-permute-start.5 = (bf16[2,1024,256]{2,1,0:T(8,128)(2,1)S(1)}, bf16[2,1024,256]{2,1,0:T(8,128)(2,1)}, u32[]{:S(2)}, u32[]{:S(2)}) collective-permute-start(bf16[2,1024,256]{2,1,0:T(8,128)(2,1)S(1)} %copy-done.1), channel_id=1, source_target_pairs={{0,4},{2,6},{4,0},{6,2},{8,12},{10,14},{12,8},{14,10},{16,20},{18,... | collective-permute-start | bytes 3145736 | tf_op jit(solution)/shard_map/ppermute | solution.py:360
  19.3 0.6 fusion.77
  20.3 0.6 exponential_bitcast_fusion
  20.9 0.6 subtract_exponential_fusion.3
  21.8 0.6 exponential_bitcast_fusion.1
  22.4 0.6 subtract_exponential_fusion.4
  23.0 0.6 iota_compare_fusion
  23.9 0.7 subtract_convert_fusion
  24.7 0.6 slice_convert_fusion.4
  25.6 0.7 pad_maximum_fusion.4
  26.3 0.8 fusion.61
  27.1 0.7 maximum_bitcast_fusion.5
  27.8 0.8 copy.123
  28.6 1.3 max.26
  29.9 0.7 copy.141
  30.6 0.7 rev.20
  31.3 0.7 copy.138
  32.0 0.6 copy.143
  33.0 0.7 copy.136
  33.8 0.6 collective-permute-start.4
  34.3 1.8 %maximum_maximum_fusion = (bf16[130,2048]{0,1:T(8,128)(2,1)S(1)}, bf16[130,2048]{0,1:T(8,128)(2,1)S(1)}) fusion(bf16[128,512]{0,1:T(8,128)(2,1)S(1)} %copy.131, bf16[128,512]{0,1:T(8,128)(2,1)S(1)} %copy.130, bf16[128,1024]{0,1:T(8,128)(2,1)S(1)} %copy.129, bf16[2,2048]{0,1:T(8,128)(2,1)} %collective-permute-done.2, bf16[2,2048]{0,1:T(8,128)(2,1)} %collective-permute-done.3), kind=kLoop, calls=%fused_computation.21 | loop fusion | flops 4259840 | bytes 1605632 | tf_op jit(solution)/shard_map/concatenate | solution.py:28
  36.2 4.5 %multiply_convert_fusion = bf16[128,2048]{0,1:T(8,128)(2,1)S(1)} fusion(bf16[130,2048]{0,1:T(8,128)(2,1)S(1)} %get-tuple-element.33, bf16[130,2048]{0,1:T(8,128)(2,1)S(1)} %get-tuple-element.32, f32[2048]{0:T(1024)S(1)} %bitcast.193, f32[2048]{0:T(1024)S(1)} %bitcast.194, f32[2048]{0:T(1024)S(1)} %bitcast.195, f32[2048]{0:T(1024)S(1)} %bitcast.196, ...), kind=kLoop, calls=%fused_computation.31 | loop fusion | flops 6291456 | bytes 3186688 | tf_op jit(solution)/shard_map/convert_element_type | solution.py:463
  43.0 0.8 maximum_bitcast_fusion.state_ref
  43.8 0.7 broadcast_in_dim.42.decay_ref
  44.5 24.9 %shard_map.154 = bf16[4,2,4,64,128]{4,3,2,1,0:T(8,128)(2,1)} custom-call(bf16[4,2,4,64,128]{4,3,2,1,0:T(8,128)(2,1)} %maximum_bitcast_fusion.state_ref, f32[4,2,4,128]{3,2,1,0:T(4,128)} %broadcast_in_dim.42.decay_ref), custom_call_target="tpu_custom_call" | custom-call | tf_op jit(solution)/shard_map/pallas_call | solution.py:222
  69.4 1.2 fusion.4
  70.6 1.3 fusion.1
  72.0 1.3 copy.153
  73.5 0.8 copy.134
  74.7 2.3 %fusion.2 = f32[1,128,4,4,64]{1,4,3,2,0:T(8,128)} fusion(f32[1,128,4,4,64]{1,4,3,2,0:T(8,128)S(1)} %fusion.3, f32[128,4,4]{0,2,1:T(4,128)S(1)} %copy-done.25, f32[128,128,4]{1,0,2:T(8,128)} %copy.134, bf16[128,4,4,64]{0,3,2,1:T(8,128)(2,1)S(1)} %bitcast.181, pred[128,128]{1,0:T(8,128)(4,1)S(1)} %copy-done.20, f32[128,4,4]{0,2,1:T(4,128)S(1)} %bitcast.201), kind=kOutput, calls=%fused_computation.9 | convolution fusion | flops 34734080 | bytes 1605632 | tf_op jit(solution)/shard_map/blsgr,bsgrp->blgrp/dot_general | solution.py:485
  77.0 1.2 copy.154
  79.6 1.0 fusion.75
  80.7 1.0 fusion.76
  82.3 2.5 %collective-permute-start.6 = (bf16[2,1024,256]{2,1,0:T(8,128)(2,1)}, bf16[2,1024,256]{2,1,0:T(8,128)(2,1)S(1)}, u32[]{:S(2)}, u32[]{:S(2)}) collective-permute-start(bf16[2,1024,256]{2,1,0:T(8,128)(2,1)} %collective-permute-done.5.rest_2_), channel_id=1, source_target_pairs={{0,2},{2,0},{4,6},{6,4},{8,10},{10,8},{12,14},{14,12},{16,18},{18,... | collective-permute-start | bytes 3145736 | tf_op jit(solution)/shard_map/ppermute | solution.py:360
  85.7 0.8 pad_maximum_fusion.2.mixed_ref
  86.6 0.7 collective-permute-done.6.rest_3_
  87.2 1.0 copy-done.2
  88.2 73.1 %shard_map.155 = bf16[4,4,64,256]{3,2,1,0:T(8,128)(2,1)} custom-call(bf16[2,128,1024]{2,1,0:T(8,128)(2,1)} %pad_maximum_fusion.2.mixed_ref, bf16[2,1024,256]{2,1,0:T(8,128)(2,1)} %rest_0_.1, bf16[2,1024,256]{2,1,0:T(8,128)(2,1)} %collective-permute-done.4.rest_1_, bf16[2,1024,256]{2,1,0:T(8,128)(2,1)} %collective-permute-done.5.rest_2_, ...), custom_call_target="tpu_custom_call" | custom-call | tf_op jit(solution)/shard_map/pallas_call | solution.py:386
  161.3 1.4 copy.157
  162.7 1.2 reshape.502
  (135 shorter events, 7.9 us)
Async XLA Ops:
  0.0 7.6 %copy-start.5 = (bf16[128,1024]{1,0:T(8,128)(2,1)S(1)}, bf16[128,1024]{1,0:T(8,128)(2,1)}, u32[]{:S(2)}) copy-start(bf16[128,1024]{1,0:T(8,128)(2,1)} %param.20) | copy-start | bytes 786436
  0.0 7.8 %copy-start.8 = (bf16[128,512]{1,0:T(8,128)(2,1)S(1)}, bf16[128,512]{1,0:T(8,128)(2,1)}, u32[]{:S(2)}) copy-start(bf16[128,512]{1,0:T(8,128)(2,1)} %param.21) | copy-start | bytes 393220
  0.0 7.9 %copy-start.9 = (bf16[128,512]{1,0:T(8,128)(2,1)S(1)}, bf16[128,512]{1,0:T(8,128)(2,1)}, u32[]{:S(2)}) copy-start(bf16[128,512]{1,0:T(8,128)(2,1)} %param.22) | copy-start | bytes 393220
  3.2 76.4 %collective-permute-start = (bf16[128,1024]{0,1:T(8,128)(2,1)}, bf16[128,1024]{0,1:T(8,128)(2,1)}, u32[]{:S(2)}, u32[]{:S(2)}) collective-permute-start(bf16[128,1024]{0,1:T(8,128)(2,1)} %pad_maximum_fusion.3), channel_id=1, source_target_pairs={{0,2},{2,4},{4,6},{6,8},{8,10},{10,12},{12,14},{14,16},{16,18},{18... | collective-permute-start | bytes 786440 | tf_op jit(solution)/shard_map/ppermute | solution.py:30
  6.3 74.4 %collective-permute-start.1 = (bf16[128,1024]{0,1:T(8,128)(2,1)}, bf16[128,1024]{0,1:T(8,128)(2,1)}, u32[]{:S(2)}, u32[]{:S(2)}) collective-permute-start(bf16[128,1024]{0,1:T(8,128)(2,1)} %pad_maximum_fusion.3), channel_id=1, source_target_pairs={{2,0},{4,2},{6,4},{8,6},{10,8},{12,10},{14,12},{16,14},{18,16},{20... | collective-permute-start | bytes 786440 | tf_op jit(solution)/shard_map/ppermute | solution.py:32
  8.0 7.9 %copy-start.1 = (bf16[2,1024,256]{2,1,0:T(8,128)(2,1)S(1)}, bf16[2,1024,256]{2,1,0:T(8,128)(2,1)}, u32[]{:S(2)}) copy-start(bf16[2,1024,256]{2,1,0:T(8,128)(2,1)} %rest_0_.1) | copy-start | bytes 3145732
  8.0 11.2 %copy-start.36 = (f32[2,16]{1,0:T(2,128)S(1)}, f32[2,16]{1,0:T(2,128)}, u32[]{:S(2)}) copy-start(f32[2,16]{1,0:T(2,128)} %param.27) | copy-start | bytes 388
  8.1 11.2 %copy-start.21 = (f32[2,16,128]{2,1,0:T(8,128)S(1)}, f32[2,16,128]{2,1,0:T(8,128)}, u32[]{:S(2)}) copy-start(f32[2,16,128]{2,1,0:T(8,128)} %param.26) | copy-start | bytes 49156
  8.1 11.2 %copy-start.22 = (f32[2,16,128]{2,1,0:T(8,128)S(1)}, f32[2,16,128]{2,1,0:T(8,128)}, u32[]{:S(2)}) copy-start(f32[2,16,128]{2,1,0:T(8,128)} %param.28) | copy-start | bytes 49156
  9.3 14.4 %copy-start.6 = (bf16[128,1024]{1,0:T(8,128)(2,1)S(1)}, bf16[128,1024]{1,0:T(8,128)(2,1)}, u32[]{:S(2)}) copy-start(bf16[128,1024]{1,0:T(8,128)(2,1)} %param.16) | copy-start | bytes 786436
  9.3 24.5 %collective-permute-start.2 = (bf16[2,2048]{0,1:T(8,128)(2,1)}, bf16[2,2048]{0,1:T(8,128)(2,1)}, u32[]{:S(2)}, u32[]{:S(2)}) collective-permute-start(bf16[2,2048]{0,1:T(8,128)(2,1)} %get-tuple-element.34), channel_id=1, source_target_pairs={{0,2},{2,4},{4,6},{6,8},{8,10},{10,12},{12,14},{14,16},{16,18},{18... | collective-permute-start | bytes 24584 | tf_op jit(solution)/shard_map/ppermute | solution.py:30
  14.6 19.7 %collective-permute-start.3 = (bf16[2,2048]{0,1:T(8,128)(2,1)}, bf16[2,2048]{0,1:T(8,128)(2,1)}, u32[]{:S(2)}, u32[]{:S(2)}) collective-permute-start(bf16[2,2048]{0,1:T(8,128)(2,1)} %get-tuple-element.40), channel_id=1, source_target_pairs={{2,0},{4,2},{6,4},{8,6},{10,8},{12,10},{14,12},{16,14},{18,16},{20... | collective-permute-start | bytes 24584 | tf_op jit(solution)/shard_map/ppermute | solution.py:32
  15.9 66.3 %collective-permute-start.5 = (bf16[2,1024,256]{2,1,0:T(8,128)(2,1)S(1)}, bf16[2,1024,256]{2,1,0:T(8,128)(2,1)}, u32[]{:S(2)}, u32[]{:S(2)}) collective-permute-start(bf16[2,1024,256]{2,1,0:T(8,128)(2,1)S(1)} %copy-done.1), channel_id=1, source_target_pairs={{0,4},{2,6},{4,0},{6,2},{8,12},{10,14},{12,8},{14,10},{16,20},{18,... | collective-permute-start | bytes 3145736 | tf_op jit(solution)/shard_map/ppermute | solution.py:360
  20.3 4.3 %copy-start.19 = (bf16[5,1024]{1,0:T(8,128)(2,1)S(1)}, bf16[5,1024]{1,0:T(8,128)(2,1)}, u32[]{:S(2)}) copy-start(bf16[5,1024]{1,0:T(8,128)(2,1)} %param.23) | copy-start | bytes 30724
  20.3 4.3 %copy-start.28 = (bf16[5,512]{1,0:T(8,128)(2,1)S(1)}, bf16[5,512]{1,0:T(8,128)(2,1)}, u32[]{:S(2)}) copy-start(bf16[5,512]{1,0:T(8,128)(2,1)} %param.24) | copy-start | bytes 15364
  20.3 4.3 %copy-start.29 = (bf16[5,512]{1,0:T(8,128)(2,1)S(1)}, bf16[5,512]{1,0:T(8,128)(2,1)}, u32[]{:S(2)}) copy-start(bf16[5,512]{1,0:T(8,128)(2,1)} %param.25) | copy-start | bytes 15364
  24.6 1.0 copy-start.4
  33.7 2.4 %copy-start.12 = (f32[1,2048]{1,0:T(1,128)S(1)}, f32[1,2048]{1,0:T(1,128)}, u32[]{:S(2)}) copy-start(f32[1,2048]{1,0:T(1,128)} %get-tuple-element.61) | copy-start | bytes 24580
  33.7 2.4 %copy-start.13 = (f32[1,2048]{1,0:T(1,128)S(1)}, f32[1,2048]{1,0:T(1,128)}, u32[]{:S(2)}) copy-start(f32[1,2048]{1,0:T(1,128)} %get-tuple-element.62) | copy-start | bytes 24580
  33.7 2.4 %copy-start.14 = (f32[1,2048]{1,0:T(1,128)S(1)}, f32[1,2048]{1,0:T(1,128)}, u32[]{:S(2)}) copy-start(f32[1,2048]{1,0:T(1,128)} %get-tuple-element.63) | copy-start | bytes 24580
  33.7 2.5 %copy-start.15 = (f32[1,2048]{1,0:T(1,128)S(1)}, f32[1,2048]{1,0:T(1,128)}, u32[]{:S(2)}) copy-start(f32[1,2048]{1,0:T(1,128)} %get-tuple-element.64) | copy-start | bytes 24580
  33.7 2.5 %copy-start.16 = (f32[1,2048]{1,0:T(1,128)S(1)}, f32[1,2048]{1,0:T(1,128)}, u32[]{:S(2)}) copy-start(f32[1,2048]{1,0:T(1,128)} %get-tuple-element.65) | copy-start | bytes 24580
  33.8 52.8 %collective-permute-start.4 = (bf16[2,1024,256]{2,1,0:T(8,128)(2,1)S(1)}, bf16[2,1024,256]{2,1,0:T(8,128)(2,1)}, u32[]{:S(2)}, u32[]{:S(2)}) collective-permute-start(bf16[2,1024,256]{2,1,0:T(8,128)(2,1)S(1)} %copy-done.1), channel_id=1, source_target_pairs={{0,2},{2,0},{4,6},{6,4},{8,10},{10,8},{12,14},{14,12},{16,18},{18,... | collective-permute-start | bytes 3145736 | tf_op jit(solution)/shard_map/ppermute | solution.py:360
  40.7 1.7 %copy-start.27 = (f32[128,4,4]{0,2,1:T(4,128)S(1)}, f32[128,4,4]{0,2,1:T(4,128)}, u32[]{:S(2)}) copy-start(f32[128,4,4]{0,2,1:T(4,128)} %copy.141) | copy-start | bytes 24580
  40.7 1.7 %copy-start.30 = (f32[128,4,4]{0,2,1:T(4,128)S(1)}, f32[128,4,4]{0,2,1:T(4,128)}, u32[]{:S(2)}) copy-start(f32[128,4,4]{0,2,1:T(4,128)} %rev.20) | copy-start | bytes 24580
  40.7 1.7 %copy-start.34 = (f32[4,4]{1,0:T(4,128)S(1)}, f32[4,4]{1,0:T(4,128)}, u32[]{:S(2)}) copy-start(f32[4,4]{1,0:T(4,128)} %get-tuple-element.50) | copy-start | bytes 196
  41.2 1.5 copy-start.26
  41.2 1.5 copy-start.31
  41.2 1.5 copy-start.35
  42.3 1.6 copy-start.18
  42.7 26.7 %copy-start.24 = (f32[4,4]{1,0:T(4,128)S(1)}, f32[4,4]{1,0:T(4,128)}, u32[]{:S(2)}) copy-start(f32[4,4]{1,0:T(4,128)} %get-tuple-element.49) | copy-start | bytes 196
  43.0 27.6 %copy-start.20 = (pred[128,128]{1,0:T(8,128)(4,1)S(1)}, pred[128,128]{1,0:T(8,128)(4,1)}, u32[]{:S(2)}) copy-start(pred[128,128]{1,0:T(8,128)(4,1)} %iota_compare_fusion) | copy-start | bytes 49156
  72.0 2.4 %copy-start = (bf16[4,2,4,64,128]{4,3,2,1,0:T(8,128)(2,1)S(1)}, bf16[4,2,4,64,128]{4,3,2,1,0:T(8,128)(2,1)}, u32[]{:S(2)}) copy-start(bf16[4,2,4,64,128]{4,3,2,1,0:T(8,128)(2,1)} %shard_map.154) | copy-start | bytes 1572868
  72.0 2.4 %copy-start.23 = (f32[4,4]{1,0:T(4,128)S(1)}, f32[4,4]{1,0:T(4,128)}, u32[]{:S(2)}) copy-start(f32[4,4]{1,0:T(4,128)} %get-tuple-element.53) | copy-start | bytes 196
  72.0 2.7 %copy-start.25 = (f32[128,4,4]{0,2,1:T(4,128)S(1)}, f32[128,4,4]{0,2,1:T(4,128)}, u32[]{:S(2)}) copy-start(f32[128,4,4]{0,2,1:T(4,128)} %copy.136) | copy-start | bytes 24580
  72.0 2.7 %copy-start.32 = (f32[1,128,16]{1,2,0:T(8,128)S(1)}, f32[1,128,16]{1,2,0:T(8,128)}, u32[]{:S(2)}) copy-start(f32[1,128,16]{1,2,0:T(8,128)} %get-tuple-element.66) | copy-start | bytes 24580
  74.7 3.6 %copy-start.3 = (bf16[128,1024]{1,0:T(8,128)(2,1)S(1)}, bf16[128,1024]{1,0:T(8,128)(2,1)}, u32[]{:S(2)}) copy-start(bf16[128,1024]{1,0:T(8,128)(2,1)} %param.19) | copy-start | bytes 786436
  78.5 0.8 copy-start.33
  79.3 2.5 %copy-start.7 = (bf16[128,8,2,64]{0,3,2,1:T(8,128)(2,1)S(1)}, bf16[128,8,2,64]{0,3,2,1:T(8,128)(2,1)}, u32[]{:S(2)}) copy-start(bf16[128,8,2,64]{0,3,2,1:T(8,128)(2,1)} %pad_maximum_fusion.4) | copy-start | bytes 786436
  79.3 2.5 %copy-start.10 = (bf16[1,128,4,128]{3,1,2,0:T(8,128)(2,1)S(1)}, bf16[1,128,4,128]{3,1,2,0:T(8,128)(2,1)}, u32[]{:S(2)}) copy-start(bf16[1,128,4,128]{3,1,2,0:T(8,128)(2,1)} %copy.123) | copy-start | bytes 393220
  79.6 2.3 %copy-start.11 = (pred[128,384]{0,1:T(8,128)(4,1)S(1)}, pred[128,384]{0,1:T(8,128)(4,1)}, u32[]{:S(2)}) copy-start(pred[128,384]{0,1:T(8,128)(4,1)} %fusion.61) | copy-start | bytes 147460
  81.7 3.0 %copy-start.17 = (f32[4,2]{1,0:T(4,128)S(1)}, f32[4,2]{1,0:T(4,128)}, u32[]{:S(2)}) copy-start(f32[4,2]{1,0:T(4,128)} %max.26) | copy-start | bytes 100
  82.3 5.0 %collective-permute-start.6 = (bf16[2,1024,256]{2,1,0:T(8,128)(2,1)}, bf16[2,1024,256]{2,1,0:T(8,128)(2,1)S(1)}, u32[]{:S(2)}, u32[]{:S(2)}) collective-permute-start(bf16[2,1024,256]{2,1,0:T(8,128)(2,1)} %collective-permute-done.5.rest_2_), channel_id=1, source_target_pairs={{0,2},{2,0},{4,6},{6,4},{8,10},{10,8},{12,14},{14,12},{16,18},{18,... | collective-permute-start | bytes 3145736 | tf_op jit(solution)/shard_map/ppermute | solution.py:360
  87.2 1.0 copy-start.2

commit v2 on v1

--- a/solution.py
+++ b/solution.py
@@ -65,7 +65,9 @@
     outer,
     state_ref,
     decay_ref,
+    weight_ref,
     out_ref,
+    onward_ref,
     near,
     near_decay,
     prefix,
@@ -79,6 +81,7 @@
     near_sems,
     far_sems,
     reply_sems,
+    ring_sems,
 ):
     me = lax.axis_index("sp")
     spot = lax.rem(me, clique)
@@ -90,6 +93,16 @@
         [{"sp": base + mate} for mate in mates]
         + [{"sp": other * clique + spot} for other in layers]
     )
+
+    ring = sending(
+        weight_ref,
+        onward_ref,
+        ring_sems.at[0],
+        ring_sems.at[1],
+        {"sp": lax.rem(layer + 1, outer) * clique + spot},
+    )
+    if outer > 1:
+        ring.start()
 
     def near_copy(mate, slot, sem_slot):
         who = {"sp": base + mate}
@@ -206,8 +219,11 @@
                 for copy in far_copy(way, other, layer):
                     copy.wait_send()
 
-
-def scan_states(states, decays):
+    if outer > 1:
+        ring.wait()
+
+
+def scan_states(states, decays, weight):
     count = lax.axis_size("sp")
     clique = clique_of(count)
     outer = count // clique
@@ -219,11 +235,18 @@
         (clique, ways, part, cols),
     )
     block = (part, rows, cols)
-    whole_out = pl.pallas_call(
+    whole_out, onward = pl.pallas_call(
         functools.partial(scan_kernel, clique, outer),
-        out_shape=jax.ShapeDtypeStruct((clique, ways) + block, jnp.bfloat16),
-        in_specs=[pl.BlockSpec(memory_space=pltpu.VMEM)] * 2,
-        out_specs=pl.BlockSpec(memory_space=pltpu.VMEM),
+        out_shape=(
+            jax.ShapeDtypeStruct((clique, ways) + block, jnp.bfloat16),
+            jax.ShapeDtypeStruct(weight.shape, weight.dtype),
+        ),
+        in_specs=[pl.BlockSpec(memory_space=pltpu.VMEM)] * 2
+        + [pl.BlockSpec(memory_space=pl.ANY)],
+        out_specs=(
+            pl.BlockSpec(memory_space=pltpu.VMEM),
+            pl.BlockSpec(memory_space=pl.ANY),
+        ),
         scratch_shapes=[
             pltpu.VMEM((clique, ways) + block, jnp.bfloat16),
             pltpu.VMEM((clique, ways, part, cols), jnp.float32),
@@ -238,20 +261,18 @@
             pltpu.SemaphoreType.DMA((4, clique)),
             pltpu.SemaphoreType.DMA((4, 2, outer)),
             pltpu.SemaphoreType.DMA((2, clique)),
+            pltpu.SemaphoreType.DMA((2,)),
         ],
         compiler_params=pltpu.CompilerParams(collective_id=1, has_side_effects=True),
-    )(states.astype(jnp.bfloat16), decays)
-    return whole_out.transpose(1, 0, 2, 3, 4).reshape(ways, heads, rows, cols)
-
-
-def project_kernel(
-    clique,
-    outer,
-    tps,
-    mixed_ref,
-    *rest,
-):
-    weight_refs = rest[:clique]
+        cost_estimate=pl.CostEstimate(
+            flops=0, bytes_accessed=320 * states.size, transcendentals=0
+        ),
+    )(states.astype(jnp.bfloat16), decays, weight)
+    return whole_out.transpose(1, 0, 2, 3, 4).reshape(ways, heads, rows, cols), onward
+
+
+def project_kernel(clique, outer, tps, mixed_ref, *rest):
+    weight_refs = rest[:outer]
     (
         out_ref,
         gathered,
@@ -261,109 +282,107 @@
         mixed_sems,
         piece_sems,
         out_sems,
-    ) = rest[clique:]
+    ) = rest[outer:]
     me = lax.axis_index("sp")
     lane = lax.axis_index("tp")
     spot = lax.rem(me, clique)
     layer = me // clique
-    layers = [lax.rem(layer + d, outer) for d in range(1, outer)]
+    base = me - spot
+    flips = list(range(1, clique))
     lanes = [lax.rem(lane + d, tps) for d in range(1, tps)]
 
-    def at_layer(other):
-        return {"sp": other * clique + spot}
-
-    greet([at_layer(other) for other in layers] + [{"tp": other} for other in lanes])
+    def at_flip(flip):
+        return {"sp": base + flipped(spot, flip)}
+
+    greet([at_flip(flip) for flip in flips] + [{"tp": other} for other in lanes])
     share = mixed_ref.shape[1] // tps
 
-    def mixed_copy(other, slot):
+    def mixed_copy(flip):
+        low = flip & -flip
+        high = flip - low
         return sending(
-            mixed_ref,
-            gathered.at[slot],
-            mixed_sems.at[0, other],
-            mixed_sems.at[1, slot],
-            at_layer(other),
-        )
-
-    def piece_copy(block, other, slot):
+            gathered.at[high] if high else mixed_ref,
+            gathered.at[flip],
+            mixed_sems.at[0, flip],
+            mixed_sems.at[1, flip],
+            at_flip(low),
+        )
+
+    def piece_copy(flip, other, slot):
         return sending(
-            partial.at[block, other],
-            pieces.at[block, slot],
-            piece_sems.at[0, block, other],
-            piece_sems.at[1, block, slot],
+            partial.at[flip, other],
+            pieces.at[flip, slot],
+            piece_sems.at[0, flip, other],
+            piece_sems.at[1, flip, slot],
             {"tp": other},
         )
 
-    def out_copy(other, slot):
+    def out_copy(flip, slot):
         return sending(
-            summed.at[other],
+            summed.at[flip],
             out_ref.at[slot],
-            out_sems.at[0, other],
-            out_sems.at[1, slot],
-            at_layer(other),
-        )
-
-    for other in layers:
-        mixed_copy(other, layer).start()
-    gathered[layer] = mixed_ref[...]
-    order = [layer] + [lax.rem(layer + outer - d, outer) for d in range(1, outer)]
-
-    def multiply(block):
-        for flip, weight_ref in enumerate(weight_refs):
-            column = flipped(spot, flip)
+            out_sems.at[0, flip],
+            out_sems.at[1, flip],
+            at_flip(flip),
+        )
+
+    for flip in reversed(flips):
+        if flip & (flip - 1) == 0:
+            mixed_copy(flip).start()
+
+    def multiply(flip):
+        source = gathered.at[flip] if flip else mixed_ref
+        for turn, weight_ref in enumerate(weight_refs):
+            column = lax.rem(layer + outer - turn, outer)
             product = jnp.dot(
-                gathered[block, 0], weight_ref[0], preferred_element_type=jnp.float32
-            ) + jnp.dot(
-                gathered[block, 1], weight_ref[1], preferred_element_type=jnp.float32
-            )
+                source[0], weight_ref[0], preferred_element_type=jnp.float32
+            ) + jnp.dot(source[1], weight_ref[1], preferred_element_type=jnp.float32)
             rounded = product.astype(jnp.bfloat16)
             for other in range(tps):
-                partial[block, other, column] = rounded[other * share : (other + 1) * share]
+                partial[flip, other, column] = rounded[other * share : (other + 1) * share]
         for other in lanes:
-            piece_copy(block, other, lane).start()
-
-    def settle(block, own):
-        total = partial[block, lane].astype(jnp.float32)
+            piece_copy(flip, other, lane).start()
+
+    def settle(flip):
+        total = partial[flip, lane].astype(jnp.float32)
         for other in lanes:
-            piece_copy(block, other, other).wait_recv()
-            total = total + pieces[block, other].astype(jnp.float32)
-        summed[block] = total.astype(jnp.bfloat16)
-        if own:
-            out_ref[layer] = summed[layer]
+            piece_copy(flip, other, other).wait_recv()
+            total = total + pieces[flip, other].astype(jnp.float32)
+        if flip:
+            summed[flip] = total.astype(jnp.bfloat16)
+            out_copy(flip, spot).start()
         else:
-            out_copy(block, layer).start()
-
-    for turn, block in enumerate(order):
-        if turn:
-            mixed_copy(block, block).wait_recv()
-        multiply(block)
-        if turn:
-            settle(order[turn - 1], turn == 1)
-    settle(order[-1], outer == 1)
-    for other in layers:
-        out_copy(other, other).wait_recv()
-    for other in layers:
-        mixed_copy(other, layer).wait_send()
-        out_copy(other, layer).wait_send()
-    for block in order:
+            out_ref[spot] = total.astype(jnp.bfloat16)
+
+    for flip in range(clique):
+        if flip:
+            mixed_copy(flip).wait_recv()
+            for further in flips:
+                if further != flip and further - (further & -further) == flip:
+                    mixed_copy(further).start()
+        multiply(flip)
+        if flip:
+            settle(flip - 1)
+    settle(clique - 1)
+    for flip in flips:
+        out_copy(flip, flipped(spot, flip)).wait_recv()
+    for flip in flips:
+        mixed_copy(flip).wait_send()
+        out_copy(flip, spot).wait_send()
+    for flip in range(clique):
         for other in lanes:
-            piece_copy(block, other, lane).wait_send()
-
-
-def clique_weights(weight):
+            piece_copy(flip, other, lane).wait_send()
+
+
+def ring_weights(held, limit=None):
     count = lax.axis_size("sp")
     clique = clique_of(count)
-    held = [weight]
-    steps = []
-    step = clique // 2
-    while step:
-        pairs = [(i, (i // clique) * clique + ((i % clique) ^ step)) for i in range(count)]
-        held = held + [lax.ppermute(block, "sp", pairs) for block in held]
-        steps = steps + [step] if steps else [step]
-        step //= 2
-    flips = [0]
-    for step in steps:
-        flips = flips + [flip ^ step for flip in flips]
-    return [block for _, block in sorted(zip(flips, held), key=lambda item: item[0])]
+    outer = count // clique
+    pairs = [(i, (i + clique) % count) for i in range(count)]
+    held = held[:outer]
+    while len(held) < min(limit or outer, outer):
+        held = held + [lax.ppermute(held[-1], "sp", pairs)]
+    return held
 
 
 def flipped(spot, flip):
@@ -383,23 +402,24 @@
     rows = mixed.shape[1]
     width = weights[0].shape[2]
     share = rows // tps
+    block = (outer, share, width)
     out = pl.pallas_call(
         functools.partial(project_kernel, clique, outer, tps),
-        out_shape=jax.ShapeDtypeStruct((outer, clique, share, width), jnp.bfloat16),
-        in_specs=[pl.BlockSpec(memory_space=pltpu.VMEM)] * (1 + clique),
+        out_shape=jax.ShapeDtypeStruct((clique,) + block, jnp.bfloat16),
+        in_specs=[pl.BlockSpec(memory_space=pltpu.VMEM)] * (1 + outer),
         out_specs=pl.BlockSpec(memory_space=pltpu.VMEM),
         scratch_shapes=[
-            pltpu.VMEM((outer,) + mixed.shape, jnp.bfloat16),
-            pltpu.VMEM((outer, tps, clique, share, width), jnp.bfloat16),
-            pltpu.VMEM((outer, tps, clique, share, width), jnp.bfloat16),
-            pltpu.VMEM((outer, clique, share, width), jnp.bfloat16),
-            pltpu.SemaphoreType.DMA((2, outer)),
-            pltpu.SemaphoreType.DMA((2, outer, tps)),
-            pltpu.SemaphoreType.DMA((2, outer)),
+            pltpu.VMEM((clique,) + mixed.shape, jnp.bfloat16),
+            pltpu.VMEM((clique, tps) + block, jnp.bfloat16),
+            pltpu.VMEM((clique, tps) + block, jnp.bfloat16),
+            pltpu.VMEM((clique,) + block, jnp.bfloat16),
+            pltpu.SemaphoreType.DMA((2, clique)),
+            pltpu.SemaphoreType.DMA((2, clique, tps)),
+            pltpu.SemaphoreType.DMA((2, clique)),
         ],
         compiler_params=pltpu.CompilerParams(collective_id=2, has_side_effects=True),
     )(mixed, *weights)
-    return out.transpose(2, 0, 1, 3).reshape(share, outer * clique * width)
+    return out.transpose(2, 1, 0, 3).reshape(share, outer * clique * width)
 
 
 def rotate(matrix, offset):
@@ -541,7 +561,7 @@
     row_count = asking_matrix.shape[0]
     offset = lax.axis_index("sp") * row_count
     seq_total = lax.axis_size("sp") * row_count
-    weights = clique_weights(final_mapping_matrix)
+    weights = ring_weights([final_mapping_matrix], 2)
     turned_queries = rotate(asking_matrix, offset)
     key_value = jnp.concatenate([rotate(matching_key_matrix, offset), carried_value_matrix], axis=1)
     raw_rows = jnp.concatenate(
@@ -553,14 +573,6 @@
     filler = jnp.zeros((SPAN - WINDOW, key_value.shape[1]), jnp.bfloat16)
     pair_band = jnp.concatenate([filler, pair_rims, filler], axis=0)
     kv_width = matching_key_matrix.shape[1]
-    attended = attend(
-        turned_queries,
-        pair_band[:, :kv_width],
-        pair_band[:, kv_width:],
-        absorber_score_vector,
-        offset,
-        seq_total,
-    )
     conved = convolve(
         raw_rims,
         jnp.concatenate(
@@ -600,10 +612,22 @@
         scan_rows[::-1], steps_rows[1][::-1], decay_rows[1][::-1], write_rows[::-1], read_rows[::-1]
     )
     heads = groups_here * per_group
-    incoming = scan_states(
+    incoming, onward = scan_states(
         jnp.stack([ahead_summary[1], back_summary[1]]).reshape(2, heads, SSD_HEAD, STATE),
         jnp.stack([ahead_summary[0], back_summary[0]]).reshape(2, heads),
-    ).reshape(2, groups_here, per_group, SSD_HEAD, STATE)
+        weights[-1],
+    )
+    weights = ring_weights(weights + [onward])
+    incoming = incoming.reshape(2, groups_here, per_group, SSD_HEAD, STATE)
+    turned_queries, incoming = lax.optimization_barrier((turned_queries, incoming))
+    attended = attend(
+        turned_queries,
+        pair_band[:, :kv_width],
+        pair_band[:, kv_width:],
+        absorber_score_vector,
+        offset,
+        seq_total,
+    )
     both_ways = finish(ahead_pieces, incoming[0].astype(jnp.float32)) + finish(
         back_pieces, incoming[1].astype(jnp.float32)
     )[::-1]

time: 164 us -> 170 us (1.037)
  Pallas kernels: 97.9 us -> 69.6 us
  waiting for transfers between devices: 0.67 us -> 21.1 us
  local copies, waits for them, and re-layouts: 24 us -> 33.6 us
  other arithmetic: 16.1 us -> 21.5 us
    pallas_call x1, Pallas kernels: 73.1 us -> 30 us  [project(): pl.pallas_call(functools.partial(project_kernel, clique, outer, tps), out...]
    ppermute x3 -> x2, waiting for transfers between devices: 0.66 us -> 21.1 us  [ring_weights(): held = held + [lax.ppermute(held[-1], 'sp', pairs)]]
    pallas_call x1, Pallas kernels: 24.9 us -> 39.6 us  [scan_states(): pl.pallas_call(functools.partial(scan_kernel, clique, outer), out_shape=(...]
    unnamed x83 -> x97, local copies, waits for them, and re-layouts: 3.9 us -> 8.1 us
    slice x4, local copies, waits for them, and re-layouts: 2.24 us -> 4.87 us  [banded(): return jnp.concatenate([stacked[:-2], stacked[1:-1], stacked[2:]], axis=1)]
    dot_general x2, matrix products: 3.68 us -> 1.1 us  [prepare(): jnp.einsum('blsgr,bsgrp->blgrp', affinity[..., None] * fading, scaled)]
    reshape x2, local copies, waits for them, and re-layouts: 2.53 us -> 0.4 us  [finish(): return joined.reshape(joined.shape[0] * SPAN, -1)]
    exp x2, local copies, waits for them, and re-layouts: 0.22 us -> 2.07 us  [finish(): jnp.exp(running)[..., None]]
  transfers between devices with their start and end apart: 7 -> 6, of which waited for: 1 -> 1; matrix products, arithmetic and copies ran while one was open for 25% -> 28% of each run, Pallas kernels for 15% -> 0%
where the time goes in v2:
time: 170 us; the launch traced here: 168 us
  Pallas kernels  69.6 us (41%)
  local copies, waits for them, and re-layouts  33.6 us (20%)
  other arithmetic  21.5 us (13%)
  waiting for transfers between devices  21.1 us (12%)
  starting transfers between devices  16.3 us (10%)
  matrix products  5.43 us (3%)
    pallas_call x1, Pallas kernels, scan_states(): pl.pallas_call(functools.partial(scan_kernel, clique, outer), out_shape=(...  39.6 us
    pallas_call x1, Pallas kernels, project(): pl.pallas_call(functools.partial(project_kernel, clique, outer, tps), out...  30 us
    ppermute x2, waiting for transfers between devices, ring_weights(): held = held + [lax.ppermute(held[-1], 'sp', pairs)]  21.1 us
    ppermute x2, starting transfers between devices, padded_2(): lax.ppermute(tail, axis, [(i, (i + 1) % count) for i in range(ends)])  8.37 us
    unnamed x97, local copies, waits for them, and re-layouts  8.1 us
    ppermute x2, starting transfers between devices, ring_weights(): held = held + [lax.ppermute(held[-1], 'sp', pairs)]  5.32 us
    slice x4, local copies, waits for them, and re-layouts, banded(): return jnp.concatenate([stacked[:-2], stacked[1:-1], stacked[2:]], axis=1)  4.87 us
    convert_element_type x1, other arithmetic, convolve(): return jax.nn.silu(summed).astype(jnp.bfloat16)  4.47 us
  transfers between devices with their start and end apart: 6, of which 1 were waited for; matrix products, arithmetic and copies ran while one was open for 28% of the time, Pallas kernels for 0%

profile of v2, /device:TPU:0, one launch (start us, length us, event | category | flops | bytes accessed | tf_op | source)
XLA Modules:
  0.0 168.3 jit_solution(916759411969696194)
XLA Ops:
  0.0 1.1 copy.118
  1.1 1.1 copy.117
  2.5 0.7 pad_maximum_fusion.3
  3.3 1.3 collective-permute-start.1
  4.5 3.7 %collective-permute-start = (bf16[128,1024]{0,1:T(8,128)(2,1)}, bf16[128,1024]{0,1:T(8,128)(2,1)}, u32[]{:S(2)}, u32[]{:S(2)}) collective-permute-start(bf16[128,1024]{0,1:T(8,128)(2,1)} %pad_maximum_fusion.3), channel_id=1, source_target_pairs={{0,2},{2,4},{4,6},{6,8},{8,10},{10,12},{12,14},{14,16},{16,18},{18... | collective-permute-start | bytes 786440 | tf_op jit(solution)/shard_map/ppermute | solution.py:30
  8.9 1.1 fusion.74
  10.0 4.6 %collective-permute-start.2 = (bf16[2,2048]{0,1:T(8,128)(2,1)}, bf16[2,2048]{0,1:T(8,128)(2,1)}, u32[]{:S(2)}, u32[]{:S(2)}) collective-permute-start(bf16[2,2048]{0,1:T(8,128)(2,1)} %get-tuple-element.49), channel_id=1, source_target_pairs={{0,2},{2,4},{4,6},{6,8},{8,10},{10,12},{12,14},{14,16},{16,18},{18... | collective-permute-start | bytes 24584 | tf_op jit(solution)/shard_map/ppermute | solution.py:30
  14.6 1.3 collective-permute-start.3
  15.9 3.3 %collective-permute-start.4 = (bf16[2,1024,256]{2,1,0:T(8,128)(2,1)S(1)}, bf16[2,1024,256]{2,1,0:T(8,128)(2,1)S(1)}, u32[]{:S(2)}, u32[]{:S(2)}) collective-permute-start(bf16[2,1024,256]{2,1,0:T(8,128)(2,1)S(1)} %copy-done.1), channel_id=1, source_target_pairs={{0,8},{2,10},{4,12},{6,14},{8,16},{10,18},{12,20},{14,22},{16,24},... | collective-permute-start | bytes 3145736 | tf_op jit(solution)/shard_map/ppermute | solution.py:384
  24.2 0.7 constant_dynamic-update-slice_fusion.2
  24.9 0.7 constant_dynamic-update-slice_fusion.1
  25.6 0.7 constant_dynamic-update-slice_fusion
  26.9 0.8 subtract_exponential_fusion.2
  27.8 1.8 %copy.123 = bf16[128,1024]{0,1:T(8,128)(2,1)} copy(bf16[128,1024]{1,0:T(8,128)(2,1)} %param.16) | data formatting | bytes 524288 | tf_op args[0]
  29.6 1.0 convert.26
  30.6 1.6 subtract_convert_fusion
  32.1 0.9 bitcast_exponential_fusion
  33.1 1.7 %pad_maximum_fusion.4 = bf16[128,8,2,64]{0,3,2,1:T(8,128)(2,1)} fusion(bf16[128,8,1,64]{0,3,2,1:T(8,128)(2,1)} %get-tuple-element.44, bf16[128,8,1,64]{0,3,2,1:T(8,128)(2,1)} %get-tuple-element.42), kind=kLoop, calls=%fused_computation.76 | loop fusion | flops 131072 | bytes 524288 | tf_op jit(solution)/shard_map/stack | solution.py:437
  34.7 0.8 fusion.61
  35.5 1.3 maximum_bitcast_fusion.5
  36.8 1.0 copy.143
  37.8 1.7 %copy.131 = f32[128,4,4]{0,2,1:T(4,128)} copy(f32[128,4,4]{2,1,0:T(4,128)} %get-tuple-element.60) | data formatting | bytes 16384 | tf_op jit(solution)/shard_map/exp | solution.py:508
  39.5 0.7 rev.20
  40.2 0.7 copy.128
  40.9 1.3 copy.133
  42.2 0.7 copy.140
  42.9 1.0 copy.150
  43.9 0.7 copy.147
  44.7 0.8 copy.121
  45.4 1.3 max.28
  46.8 1.8 %maximum_maximum_fusion = (bf16[130,2048]{0,1:T(8,128)(2,1)S(1)}, bf16[130,2048]{0,1:T(8,128)(2,1)S(1)}) fusion(bf16[128,512]{0,1:T(8,128)(2,1)S(1)} %copy.127, bf16[128,512]{0,1:T(8,128)(2,1)S(1)} %copy.126, bf16[128,1024]{0,1:T(8,128)(2,1)S(1)} %copy.125, bf16[2,2048]{0,1:T(8,128)(2,1)} %collective-permute-done.2, bf16[2,2048]{0,1:T(8,128)(2,1)} %collective-permute-done.3), kind=kLoop, calls=%fused_computation.21 | loop fusion | flops 4259840 | bytes 1605632 | tf_op jit(solution)/shard_map/concatenate | solution.py:28
  48.7 4.5 %multiply_convert_fusion = bf16[128,2048]{0,1:T(8,128)(2,1)S(1)} fusion(bf16[130,2048]{0,1:T(8,128)(2,1)S(1)} %get-tuple-element.48, bf16[130,2048]{0,1:T(8,128)(2,1)S(1)} %get-tuple-element.47, f32[2048]{0:T(1024)S(1)} %bitcast.194, f32[2048]{0:T(1024)S(1)} %bitcast.195, f32[2048]{0:T(1024)S(1)} %bitcast.196, f32[2048]{0:T(1024)S(1)} %bitcast.197, ...), kind=kLoop, calls=%fused_computation.31 | loop fusion | flops 6291456 | bytes 3186688 | tf_op jit(solution)/shard_map/convert_element_type | solution.py:483
  56.0 0.8 maximum_bitcast_fusion.state_ref
  57.0 0.8 copy.146
  57.8 1.7 fusion.76
  59.5 0.8 copy.122
  60.3 1.7 fusion.75
  61.9 0.8 copy.120
  62.7 0.8 broadcast_in_dim.37.decay_ref
  63.7 39.6 %shard_map.154 = (bf16[4,2,4,64,128]{4,3,2,1,0:T(8,128)(2,1)}, bf16[2,1024,256]{2,1,0:T(8,128)(2,1)}) custom-call(bf16[4,2,4,64,128]{4,3,2,1,0:T(8,128)(2,1)} %maximum_bitcast_fusion.state_ref, f32[4,2,4,128]{3,2,1,0:T(4,128)} %broadcast_in_dim.37.decay_ref, bf16[2,1024,256]{2,1,0:T(8,128)(2,1)} %copy-done), custom_call_target="tpu_custom_call" | custom-call | bytes 83886080 | tf_op jit(solution)/shard_map/pallas_call | solution.py:238
  103.4 1.2 fusion.3
  108.3 2.0 %collective-permute-start.5 = (bf16[2,1024,256]{2,1,0:T(8,128)(2,1)S(1)}, bf16[2,1024,256]{2,1,0:T(8,128)(2,1)}, u32[]{:S(2)}, u32[]{:S(2)}) collective-permute-start(bf16[2,1024,256]{2,1,0:T(8,128)(2,1)S(1)} %copy-done.2), channel_id=1, source_target_pairs={{0,8},{2,10},{4,12},{6,14},{8,16},{10,18},{12,20},{14,22},{16,24},... | collective-permute-start | bytes 3145736 | tf_op jit(solution)/shard_map/ppermute | solution.py:384
  110.3 1.5 fusion.79
  113.7 0.8 pad_maximum_fusion.2.mixed_ref
  114.6 21.1 %collective-permute-done.5.rest_3_ = bf16[2,1024,256]{2,1,0:T(8,128)(2,1)} collective-permute-done((bf16[2,1024,256]{2,1,0:T(8,128)(2,1)S(1)}, bf16[2,1024,256]{2,1,0:T(8,128)(2,1)}, u32[]{:S(2)}, u32[]{:S(2)}) %collective-permute-start.5) | collective-permute-done | bytes 1048608 | tf_op jit(solution)/shard_map/ppermute | solution.py:384
  135.6 30.0 %shard_map.155 = bf16[4,4,64,256]{3,2,1,0:T(8,128)(2,1)} custom-call(bf16[2,128,1024]{2,1,0:T(8,128)(2,1)} %pad_maximum_fusion.2.mixed_ref, bf16[2,1024,256]{2,1,0:T(8,128)(2,1)} %rest_0_.1, bf16[2,1024,256]{2,1,0:T(8,128)(2,1)} %copy-done, bf16[2,1024,256]{2,1,0:T(8,128)(2,1)} %get-tuple-element.40.rest_2_, bf16[2,1024,256]{2,1,0:T(8,128)(2,1)} %collective-permute-done.5.rest_3_), custom_call_target="tpu_custom_call" | custom-call | tf_op jit(solution)/shard_map/pallas_call | solution.py:406
  165.6 1.4 copy.155
  167.1 1.2 reshape.504
  (147 shorter events, 14.8 us)
Async XLA Ops:
  0.0 8.3 %copy-start.13 = (bf16[128,512]{1,0:T(8,128)(2,1)S(1)}, bf16[128,512]{1,0:T(8,128)(2,1)}, u32[]{:S(2)}) copy-start(bf16[128,512]{1,0:T(8,128)(2,1)} %param.22) | copy-start | bytes 393220
  0.0 8.4 %copy-start.14 = (bf16[128,512]{1,0:T(8,128)(2,1)S(1)}, bf16[128,512]{1,0:T(8,128)(2,1)}, u32[]{:S(2)}) copy-start(bf16[128,512]{1,0:T(8,128)(2,1)} %param.21) | copy-start | bytes 393220
  0.0 8.6 %copy-start.9 = (bf16[128,1024]{1,0:T(8,128)(2,1)S(1)}, bf16[128,1024]{1,0:T(8,128)(2,1)}, u32[]{:S(2)}) copy-start(bf16[128,1024]{1,0:T(8,128)(2,1)} %param.20) | copy-start | bytes 786436
  1.1 3.4 %copy-start.5 = (bf16[128,512]{0,1:T(8,128)(2,1)}, bf16[128,512]{0,1:T(8,128)(2,1)S(1)}, u32[]{:S(2)}) copy-start(bf16[128,512]{0,1:T(8,128)(2,1)S(1)} %copy.118) | copy-start | bytes 393220
  2.4 6.1 %copy-start.7 = (f32[128,64]{0,1:T(8,128)}, f32[128,64]{0,1:T(8,128)S(1)}, u32[]{:S(2)}) copy-start(f32[128,64]{0,1:T(8,128)S(1)} %get-tuple-element.80) | copy-start | bytes 98308
  2.4 6.1 %copy-start.8 = (f32[128,64]{0,1:T(8,128)}, f32[128,64]{0,1:T(8,128)S(1)}, u32[]{:S(2)}) copy-start(f32[128,64]{0,1:T(8,128)S(1)} %get-tuple-element.81) | copy-start | bytes 98308
  3.3 54.6 %collective-permute-start.1 = (bf16[128,1024]{0,1:T(8,128)(2,1)}, bf16[128,1024]{0,1:T(8,128)(2,1)}, u32[]{:S(2)}, u32[]{:S(2)}) collective-permute-start(bf16[128,1024]{0,1:T(8,128)(2,1)} %pad_maximum_fusion.3), channel_id=1, source_target_pairs={{2,0},{4,2},{6,4},{8,6},{10,8},{12,10},{14,12},{16,14},{18,16},{20... | collective-permute-start | bytes 786440 | tf_op jit(solution)/shard_map/ppermute | solution.py:32
  4.5 55.7 %collective-permute-start = (bf16[128,1024]{0,1:T(8,128)(2,1)}, bf16[128,1024]{0,1:T(8,128)(2,1)}, u32[]{:S(2)}, u32[]{:S(2)}) collective-permute-start(bf16[128,1024]{0,1:T(8,128)(2,1)} %pad_maximum_fusion.3), channel_id=1, source_target_pairs={{0,2},{2,4},{4,6},{6,8},{8,10},{10,12},{12,14},{14,16},{16,18},{18... | collective-permute-start | bytes 786440 | tf_op jit(solution)/shard_map/ppermute | solution.py:30
  8.8 7.2 %copy-start.1 = (bf16[2,1024,256]{2,1,0:T(8,128)(2,1)S(1)}, bf16[2,1024,256]{2,1,0:T(8,128)(2,1)}, u32[]{:S(2)}) copy-start(bf16[2,1024,256]{2,1,0:T(8,128)(2,1)} %rest_0_.1) | copy-start | bytes 3145732
  8.8 10.5 %copy-start.43 = (f32[2,16]{1,0:T(2,128)S(1)}, f32[2,16]{1,0:T(2,128)}, u32[]{:S(2)}) copy-start(f32[2,16]{1,0:T(2,128)} %param.27) | copy-start | bytes 388
  8.8 10.5 %copy-start.27 = (f32[2,16,128]{2,1,0:T(8,128)S(1)}, f32[2,16,128]{2,1,0:T(8,128)}, u32[]{:S(2)}) copy-start(f32[2,16,128]{2,1,0:T(8,128)} %param.26) | copy-start | bytes 49156
  8.8 10.5 %copy-start.28 = (f32[2,16,128]{2,1,0:T(8,128)S(1)}, f32[2,16,128]{2,1,0:T(8,128)}, u32[]{:S(2)}) copy-start(f32[2,16,128]{2,1,0:T(8,128)} %param.28) | copy-start | bytes 49156
  10.0 36.8 %collective-permute-start.2 = (bf16[2,2048]{0,1:T(8,128)(2,1)}, bf16[2,2048]{0,1:T(8,128)(2,1)}, u32[]{:S(2)}, u32[]{:S(2)}) collective-permute-start(bf16[2,2048]{0,1:T(8,128)(2,1)} %get-tuple-element.49), channel_id=1, source_target_pairs={{0,2},{2,4},{4,6},{6,8},{8,10},{10,12},{12,14},{14,16},{16,18},{18... | collective-permute-start | bytes 24584 | tf_op jit(solution)/shard_map/ppermute | solution.py:30
  14.6 32.2 %collective-permute-start.3 = (bf16[2,2048]{0,1:T(8,128)(2,1)}, bf16[2,2048]{0,1:T(8,128)(2,1)}, u32[]{:S(2)}, u32[]{:S(2)}) collective-permute-start(bf16[2,2048]{0,1:T(8,128)(2,1)} %get-tuple-element.50), channel_id=1, source_target_pairs={{2,0},{4,2},{6,4},{8,6},{10,8},{12,10},{14,12},{16,14},{18,16},{20... | collective-permute-start | bytes 24584 | tf_op jit(solution)/shard_map/ppermute | solution.py:32
  15.9 46.8 %collective-permute-start.4 = (bf16[2,1024,256]{2,1,0:T(8,128)(2,1)S(1)}, bf16[2,1024,256]{2,1,0:T(8,128)(2,1)S(1)}, u32[]{:S(2)}, u32[]{:S(2)}) collective-permute-start(bf16[2,1024,256]{2,1,0:T(8,128)(2,1)S(1)} %copy-done.1), channel_id=1, source_target_pairs={{0,8},{2,10},{4,12},{6,14},{8,16},{10,18},{12,20},{14,22},{16,24},... | collective-permute-start | bytes 3145736 | tf_op jit(solution)/shard_map/ppermute | solution.py:384
  29.5 5.2 %copy-start.35 = (s32[384]{0:T(512)S(1)}, s32[384]{0:T(512)}, u32[]{:S(2)}) copy-start(s32[384]{0:T(512)} %iota_add_fusion.1) | copy-start | bytes 4612
  46.8 1.9 %copy-start.18 = (f32[1,2048]{1,0:T(1,128)S(1)}, f32[1,2048]{1,0:T(1,128)}, u32[]{:S(2)}) copy-start(f32[1,2048]{1,0:T(1,128)} %get-tuple-element.69) | copy-start | bytes 24580
  46.8 1.9 %copy-start.19 = (f32[1,2048]{1,0:T(1,128)S(1)}, f32[1,2048]{1,0:T(1,128)}, u32[]{:S(2)}) copy-start(f32[1,2048]{1,0:T(1,128)} %get-tuple-element.70) | copy-start | bytes 24580
  46.8 1.9 %copy-start.20 = (f32[1,2048]{1,0:T(1,128)S(1)}, f32[1,2048]{1,0:T(1,128)}, u32[]{:S(2)}) copy-start(f32[1,2048]{1,0:T(1,128)} %get-tuple-element.71) | copy-start | bytes 24580
  46.8 1.9 %copy-start.21 = (f32[1,2048]{1,0:T(1,128)S(1)}, f32[1,2048]{1,0:T(1,128)}, u32[]{:S(2)}) copy-start(f32[1,2048]{1,0:T(1,128)} %get-tuple-element.72) | copy-start | bytes 24580
  46.8 1.9 %copy-start.22 = (f32[1,2048]{1,0:T(1,128)S(1)}, f32[1,2048]{1,0:T(1,128)}, u32[]{:S(2)}) copy-start(f32[1,2048]{1,0:T(1,128)} %get-tuple-element.73) | copy-start | bytes 24580
  53.2 2.0 %copy-start.34 = (f32[128,4,4]{0,2,1:T(4,128)S(1)}, f32[128,4,4]{0,2,1:T(4,128)}, u32[]{:S(2)}) copy-start(f32[128,4,4]{0,2,1:T(4,128)} %copy.131) | copy-start | bytes 24580
  53.2 2.0 %copy-start.36 = (f32[128,4,4]{0,2,1:T(4,128)S(1)}, f32[128,4,4]{0,2,1:T(4,128)}, u32[]{:S(2)}) copy-start(f32[128,4,4]{0,2,1:T(4,128)} %rev.20) | copy-start | bytes 24580
  53.2 2.0 %copy-start.42 = (f32[4,4]{1,0:T(4,128)S(1)}, f32[4,4]{1,0:T(4,128)}, u32[]{:S(2)}) copy-start(f32[4,4]{1,0:T(4,128)} %get-tuple-element.58) | copy-start | bytes 196
  53.2 2.5 %copy-start.33 = (f32[128,4,4]{0,2,1:T(4,128)S(1)}, f32[128,4,4]{0,2,1:T(4,128)}, u32[]{:S(2)}) copy-start(f32[128,4,4]{0,2,1:T(4,128)} %copy.128) | copy-start | bytes 24580
  53.3 2.5 %copy-start.38 = (f32[1,128,16]{1,2,0:T(8,128)S(1)}, f32[1,128,16]{1,2,0:T(8,128)}, u32[]{:S(2)}) copy-start(f32[1,128,16]{1,2,0:T(8,128)} %get-tuple-element.74) | copy-start | bytes 24580
  53.3 2.5 %copy-start.41 = (f32[4,4]{1,0:T(4,128)S(1)}, f32[4,4]{1,0:T(4,128)}, u32[]{:S(2)}) copy-start(f32[4,4]{1,0:T(4,128)} %get-tuple-element.65) | copy-start | bytes 196
  57.0 5.7 %copy-start.24 = (f32[4,2,4]{2,1,0:T(2,128)S(1)}, f32[4,2,4]{2,1,0:T(2,128)}, u32[]{:S(2)}) copy-start(f32[4,2,4]{2,1,0:T(2,128)} %copy.133) | copy-start | bytes 388
  57.8 45.5 %copy-start.30 = (f32[4,4]{1,0:T(4,128)S(1)}, f32[4,4]{1,0:T(4,128)}, u32[]{:S(2)}) copy-start(f32[4,4]{1,0:T(4,128)} %get-tuple-element.66) | copy-start | bytes 196
  60.2 44.4 %copy-start.25 = (pred[128,128]{1,0:T(8,128)(4,1)S(1)}, pred[128,128]{1,0:T(8,128)(4,1)}, u32[]{:S(2)}) copy-start(pred[128,128]{1,0:T(8,128)(4,1)} %iota_compare_fusion) | copy-start | bytes 49156
  60.2 44.4 %copy-start.32 = (f32[128,4,4]{0,2,1:T(4,128)S(1)}, f32[128,4,4]{0,2,1:T(4,128)}, u32[]{:S(2)}) copy-start(f32[128,4,4]{0,2,1:T(4,128)} %copy.140) | copy-start | bytes 24580
  60.2 44.4 %copy-start.39 = (f32[1,128,16]{1,2,0:T(8,128)S(1)}, f32[1,128,16]{1,2,0:T(8,128)}, u32[]{:S(2)}) copy-start(f32[1,128,16]{1,2,0:T(8,128)} %get-tuple-element.74) | copy-start | bytes 24580
  62.7 1.0 copy-start
  104.6 1.0 copy-start.4
  104.6 1.0 copy-start.29
  104.6 1.3 copy-start.11
  104.7 1.3 copy-start.12
  104.7 1.3 copy-start.26
  104.7 1.3 copy-start.31
  104.7 1.3 copy-start.37
  106.0 1.0 copy-start.3
  107.0 1.2 copy-start.2
  107.0 3.2 %copy-start.15 = (bf16[1,128,4,128]{3,1,2,0:T(8,128)(2,1)S(1)}, bf16[1,128,4,128]{3,1,2,0:T(8,128)(2,1)}, u32[]{:S(2)}) copy-start(bf16[1,128,4,128]{3,1,2,0:T(8,128)(2,1)} %copy.121) | copy-start | bytes 393220
  107.7 4.0 %copy-start.23 = (f32[4,2]{1,0:T(4,128)S(1)}, f32[4,2]{1,0:T(4,128)}, u32[]{:S(2)}) copy-start(f32[4,2]{1,0:T(4,128)} %max.28) | copy-start | bytes 100
  108.3 27.4 %collective-permute-start.5 = (bf16[2,1024,256]{2,1,0:T(8,128)(2,1)S(1)}, bf16[2,1024,256]{2,1,0:T(8,128)(2,1)}, u32[]{:S(2)}, u32[]{:S(2)}) collective-permute-start(bf16[2,1024,256]{2,1,0:T(8,128)(2,1)S(1)} %copy-done.2), channel_id=1, source_target_pairs={{0,8},{2,10},{4,12},{6,14},{8,16},{10,18},{12,20},{14,22},{16,24},... | collective-permute-start | bytes 3145736 | tf_op jit(solution)/shard_map/ppermute | solution.py:384
  111.8 0.9 copy-start.6
  111.8 1.0 copy-start.16
  111.8 1.0 copy-start.17
  (2 other events, 1.4 us)

commit v3 on v2

--- a/solution.py
+++ b/solution.py
@@ -272,7 +272,8 @@
 
 
 def project_kernel(clique, outer, tps, mixed_ref, *rest):
-    weight_refs = rest[:outer]
+    given = max(outer - 1, 1)
+    weight_refs = list(rest[:given])
     (
         out_ref,
         gathered,
@@ -282,7 +283,9 @@
         mixed_sems,
         piece_sems,
         out_sems,
-    ) = rest[outer:]
+        last,
+        ring_sems,
+    ) = rest[given:]
     me = lax.axis_index("sp")
     lane = lax.axis_index("tp")
     spot = lax.rem(me, clique)
@@ -294,7 +297,17 @@
     def at_flip(flip):
         return {"sp": base + flipped(spot, flip)}
 
-    greet([at_flip(flip) for flip in flips] + [{"tp": other} for other in lanes])
+    after = {"sp": lax.rem(layer + 1, outer) * clique + spot}
+    prior = {"sp": lax.rem(layer + outer - 1, outer) * clique + spot}
+    greet(
+        [at_flip(flip) for flip in flips]
+        + [{"tp": other} for other in lanes]
+        + ([after, prior] if outer > 1 else [])
+    )
+    ring = sending(weight_refs[-1], last, ring_sems.at[0], ring_sems.at[1], after)
+    if outer > 1:
+        ring.start()
+        weight_refs = weight_refs + [last]
     share = mixed_ref.shape[1] // tps
 
     def mixed_copy(flip):
@@ -330,9 +343,10 @@
         if flip & (flip - 1) == 0:
             mixed_copy(flip).start()
 
-    def multiply(flip):
+    def multiply(flip, turns):
         source = gathered.at[flip] if flip else mixed_ref
-        for turn, weight_ref in enumerate(weight_refs):
+        for turn in turns:
+            weight_ref = weight_refs[turn]
             column = lax.rem(layer + outer - turn, outer)
             product = jnp.dot(
                 source[0], weight_ref[0], preferred_element_type=jnp.float32
@@ -340,8 +354,6 @@
             rounded = product.astype(jnp.bfloat16)
             for other in range(tps):
                 partial[flip, other, column] = rounded[other * share : (other + 1) * share]
-        for other in lanes:
-            piece_copy(flip, other, lane).start()
 
     def settle(flip):
         total = partial[flip, lane].astype(jnp.float32)
@@ -360,7 +372,13 @@
             for further in flips:
                 if further != flip and further - (further & -further) == flip:
                     mixed_copy(further).start()
-        multiply(flip)
+        multiply(flip, range(given))
+    if outer > 1:
+        ring.wait_recv()
+    for flip in range(clique):
+        multiply(flip, range(given, outer))
+        for other in lanes:
+            piece_copy(flip, other, lane).start()
         if flip:
             settle(flip - 1)
     settle(clique - 1)
@@ -372,15 +390,18 @@
     for flip in range(clique):
         for other in lanes:
             piece_copy(flip, other, lane).wait_send()
-
-
-def ring_weights(held, limit=None):
+    if outer > 1:
+        ring.wait_send()
+
+
+def ring_weights(held, limit):
     count = lax.axis_size("sp")
     clique = clique_of(count)
     outer = count // clique
     pairs = [(i, (i + clique) % count) for i in range(count)]
-    held = held[:outer]
-    while len(held) < min(limit or outer, outer):
+    goal = max(outer + limit, 1) if limit < 0 else min(limit, outer)
+    held = held[: max(outer - 1, 1)]
+    while len(held) < goal:
         held = held + [lax.ppermute(held[-1], "sp", pairs)]
     return held
 
@@ -406,7 +427,7 @@
     out = pl.pallas_call(
         functools.partial(project_kernel, clique, outer, tps),
         out_shape=jax.ShapeDtypeStruct((clique,) + block, jnp.bfloat16),
-        in_specs=[pl.BlockSpec(memory_space=pltpu.VMEM)] * (1 + outer),
+        in_specs=[pl.BlockSpec(memory_space=pltpu.VMEM)] * (1 + len(weights)),
         out_specs=pl.BlockSpec(memory_space=pltpu.VMEM),
         scratch_shapes=[
             pltpu.VMEM((clique,) + mixed.shape, jnp.bfloat16),
@@ -416,6 +437,8 @@
             pltpu.SemaphoreType.DMA((2, clique)),
             pltpu.SemaphoreType.DMA((2, clique, tps)),
             pltpu.SemaphoreType.DMA((2, clique)),
+            pltpu.VMEM(weights[0].shape, weights[0].dtype),
+            pltpu.SemaphoreType.DMA((2,)),
         ],
         compiler_params=pltpu.CompilerParams(collective_id=2, has_side_effects=True),
     )(mixed, *weights)
@@ -617,7 +640,7 @@
         jnp.stack([ahead_summary[0], back_summary[0]]).reshape(2, heads),
         weights[-1],
     )
-    weights = ring_weights(weights + [onward])
+    weights = ring_weights(weights + [onward], -1)
     incoming = incoming.reshape(2, groups_here, per_group, SSD_HEAD, STATE)
     turned_queries, incoming = lax.optimization_barrier((turned_queries, incoming))
     attended = attend(

time: 170 us -> 149 us (0.88)
  waiting for transfers between devices: 21.1 us -> 2.67 us
  Pallas kernels: 69.6 us -> 86.8 us
  local copies, waits for them, and re-layouts: 33.6 us -> 21.3 us
  other arithmetic: 21.5 us -> 17.6 us
  starting transfers between devices: 16.3 us -> 14.4 us
    pallas_call x1, Pallas kernels: 30 us -> 49.7 us  [project(): pl.pallas_call(functools.partial(project_kernel, clique, outer, tps), out...]
    ppermute x2 -> x1, waiting for transfers between devices: 21.1 us -> 2.66 us  [ring_weights(): held = held + [lax.ppermute(held[-1], 'sp', pairs)]]
    unnamed x97 -> x85, local copies, waits for them, and re-layouts: 8.1 us -> 3.82 us
    pallas_call x1, Pallas kernels: 39.6 us -> 37.2 us  [scan_states(): pl.pallas_call(functools.partial(scan_kernel, clique, outer), out_shape=(...]
    exp x2, local copies, waits for them, and re-layouts: 2.4 us -> 0.25 us  [prepare(): to_end = jnp.exp(running[:, -1:] - running)]
    ppermute x2 -> x1, starting transfers between devices: 5.32 us -> 3.29 us  [ring_weights(): held = held + [lax.ppermute(held[-1], 'sp', pairs)]]
    exp x2, local copies, waits for them, and re-layouts: 2.07 us -> 0.19 us  [finish(): jnp.exp(running)[..., None]]
  transfers between devices with their start and end apart: 6 -> 5, of which waited for: 1 -> 1; matrix products, arithmetic and copies ran while one was open for 28% -> 20% of each run, Pallas kernels for 0% -> 0%
where the time goes in v3:
time: 149 us; the launch traced here: 148 us
  Pallas kernels  86.8 us (58%)
  local copies, waits for them, and re-layouts  21.3 us (14%)
  other arithmetic  17.6 us (12%)
  starting transfers between devices  14.4 us (10%)
  matrix products  4.35 us (3%)
  waiting for transfers between devices  2.67 us (2%)
    pallas_call x1, Pallas kernels, project(): pl.pallas_call(functools.partial(project_kernel, clique, outer, tps), out...  49.7 us
    pallas_call x1, Pallas kernels, scan_states(): pl.pallas_call(functools.partial(scan_kernel, clique, outer), out_shape=(...  37.2 us
    ppermute x2, starting transfers between devices, padded_2(): lax.ppermute(tail, axis, [(i, (i + 1) % count) for i in range(ends)])  8.55 us
    convert_element_type x1, other arithmetic, convolve(): return jax.nn.silu(summed).astype(jnp.bfloat16)  4.47 us
    slice x4, local copies, waits for them, and re-layouts, banded(): return jnp.concatenate([stacked[:-2], stacked[1:-1], stacked[2:]], axis=1)  4.14 us
    unnamed x85, local copies, waits for them, and re-layouts  3.82 us
    ppermute x1, starting transfers between devices, ring_weights(): held = held + [lax.ppermute(held[-1], 'sp', pairs)]  3.29 us
  transfers between devices with their start and end apart: 5, of which 1 were waited for; matrix products, arithmetic and copies ran while one was open for 20% of the time, Pallas kernels for 0%

profile of v3, /device:TPU:0, one launch (start us, length us, event | category | flops | bytes accessed | tf_op | source)
XLA Modules:
  0.0 147.9 jit_solution(12837175990119012125)
XLA Ops:
  0.0 1.1 copy.118
  1.1 1.0 copy.117
  2.4 0.7 pad_maximum_fusion.3
  3.2 1.3 collective-permute-start.1
  4.5 3.8 %collective-permute-start = (bf16[128,1024]{0,1:T(8,128)(2,1)}, bf16[128,1024]{0,1:T(8,128)(2,1)}, u32[]{:S(2)}, u32[]{:S(2)}) collective-permute-start(bf16[128,1024]{0,1:T(8,128)(2,1)} %pad_maximum_fusion.3), channel_id=1, source_target_pairs={{0,2},{2,4},{4,6},{6,8},{8,10},{10,12},{12,14},{14,16},{16,18},{18... | collective-permute-start | bytes 786440 | tf_op jit(solution)/shard_map/ppermute | solution.py:30
  8.7 1.1 fusion.74
  9.9 4.8 %collective-permute-start.2 = (bf16[2,2048]{0,1:T(8,128)(2,1)}, bf16[2,2048]{0,1:T(8,128)(2,1)}, u32[]{:S(2)}, u32[]{:S(2)}) collective-permute-start(bf16[2,2048]{0,1:T(8,128)(2,1)} %get-tuple-element.49), channel_id=1, source_target_pairs={{0,2},{2,4},{4,6},{6,8},{8,10},{10,12},{12,14},{14,16},{16,18},{18... | collective-permute-start | bytes 24584 | tf_op jit(solution)/shard_map/ppermute | solution.py:30
  14.7 1.3 collective-permute-start.3
  16.0 3.3 %collective-permute-start.4 = (bf16[2,1024,256]{2,1,0:T(8,128)(2,1)}, bf16[2,1024,256]{2,1,0:T(8,128)(2,1)S(1)}, u32[]{:S(2)}, u32[]{:S(2)}) collective-permute-start(bf16[2,1024,256]{2,1,0:T(8,128)(2,1)} %rest_0_.1), channel_id=1, source_target_pairs={{0,8},{2,10},{4,12},{6,14},{8,16},{10,18},{12,20},{14,22},{16,24},... | collective-permute-start | bytes 3145736 | tf_op jit(solution)/shard_map/ppermute | solution.py:405
  19.4 0.6 fusion.77
  20.3 0.6 exponential_bitcast_fusion.1
  20.9 0.6 exponential_multiply_fusion.1
  21.8 0.6 exponential_bitcast_fusion
  22.4 0.6 subtract_exponential_fusion.3
  23.0 0.6 iota_compare_fusion
  23.6 0.6 iota_add_fusion.1
  24.2 0.6 slice_convert_fusion.4
  25.2 0.7 subtract_convert_fusion
  26.1 1.6 %pad_maximum_fusion.4 = bf16[128,8,2,64]{0,3,2,1:T(8,128)(2,1)} fusion(bf16[128,8,1,64]{0,3,2,1:T(8,128)(2,1)} %get-tuple-element.44, bf16[128,8,1,64]{0,3,2,1:T(8,128)(2,1)S(1)} %get-tuple-element.42), kind=kLoop, calls=%fused_computation.76 | loop fusion | flops 131072 | bytes 524288 | tf_op jit(solution)/shard_map/stack | solution.py:460
  27.8 0.8 fusion.61
  28.6 0.7 maximum_bitcast_fusion.5
  29.7 0.6 copy.133
  30.3 0.7 copy.140
  31.1 0.7 copy.147
  32.0 1.3 max.28
  33.4 1.8 %maximum_maximum_fusion = (bf16[130,2048]{0,1:T(8,128)(2,1)S(1)}, bf16[130,2048]{0,1:T(8,128)(2,1)S(1)}) fusion(bf16[128,512]{0,1:T(8,128)(2,1)S(1)} %copy.127, bf16[128,512]{0,1:T(8,128)(2,1)S(1)} %copy.126, bf16[128,1024]{0,1:T(8,128)(2,1)S(1)} %copy.125, bf16[2,2048]{0,1:T(8,128)(2,1)} %collective-permute-done.2, bf16[2,2048]{0,1:T(8,128)(2,1)} %collective-permute-done.3), kind=kLoop, calls=%fused_computation.21 | loop fusion | flops 4259840 | bytes 1605632 | tf_op jit(solution)/shard_map/concatenate | solution.py:28
  35.3 4.5 %multiply_convert_fusion = bf16[128,2048]{0,1:T(8,128)(2,1)S(1)} fusion(bf16[130,2048]{0,1:T(8,128)(2,1)S(1)} %get-tuple-element.48, bf16[130,2048]{0,1:T(8,128)(2,1)S(1)} %get-tuple-element.47, f32[2048]{0:T(1024)S(1)} %bitcast.194, f32[2048]{0:T(1024)S(1)} %bitcast.195, f32[2048]{0:T(1024)S(1)} %bitcast.196, f32[2048]{0:T(1024)S(1)} %bitcast.197, ...), kind=kLoop, calls=%fused_computation.31 | loop fusion | flops 6291456 | bytes 3186688 | tf_op jit(solution)/shard_map/convert_element_type | solution.py:506
  39.8 0.4 rev.21
  40.5 0.4 rev.22
  41.9 0.8 maximum_bitcast_fusion.state_ref
  43.0 1.6 %fusion.76 = (bf16[128,512]{0,1:T(8,128)(2,1)}, bf16[128,512]{0,1:T(8,128)(2,1)S(1)}) fusion(bf16[128,1024]{0,1:T(8,128)(2,1)} %collective-permute-done.1), kind=kLoop, calls=%fused_computation.143 | loop fusion | bytes 524288 | tf_op jit(solution)/shard_map/slice | solution.py:468
  44.8 1.6 %fusion.75 = (bf16[128,512]{0,1:T(8,128)(2,1)}, bf16[128,512]{0,1:T(8,128)(2,1)S(1)}) fusion(bf16[128,1024]{0,1:T(8,128)(2,1)} %collective-permute-done), kind=kLoop, calls=%fused_computation.142 | loop fusion | bytes 524288 | tf_op jit(solution)/shard_map/slice | solution.py:468
  46.4 0.8 copy.120
  47.2 2.7 %collective-permute-done.4.weight_ref.rest_1_ = bf16[2,1024,256]{2,1,0:T(8,128)(2,1)S(1)} collective-permute-done((bf16[2,1024,256]{2,1,0:T(8,128)(2,1)}, bf16[2,1024,256]{2,1,0:T(8,128)(2,1)S(1)}, u32[]{:S(2)}, u32[]{:S(2)}) %collective-permute-start.4) | collective-permute-done | bytes 1048608 | tf_op jit(solution)/shard_map/ppermute | solution.py:405
  49.8 0.8 broadcast_in_dim.37.decay_ref
  50.6 0.2 copy-done
  50.9 37.2 %shard_map.154 = (bf16[4,2,4,64,128]{4,3,2,1,0:T(8,128)(2,1)}, bf16[2,1024,256]{2,1,0:T(8,128)(2,1)}) custom-call(bf16[4,2,4,64,128]{4,3,2,1,0:T(8,128)(2,1)} %maximum_bitcast_fusion.state_ref, f32[4,2,4,128]{3,2,1,0:T(4,128)} %broadcast_in_dim.37.decay_ref, bf16[2,1024,256]{2,1,0:T(8,128)(2,1)} %copy-done), custom_call_target="tpu_custom_call" | custom-call | bytes 83886080 | tf_op jit(solution)/shard_map/pallas_call | solution.py:238
  88.0 1.2 fusion.3
  89.3 0.5 fusion.2
  90.3 0.3 fusion.4
  90.7 0.6 fusion.1
  91.9 0.2 mul.423
  92.9 0.4 fusion.79
  93.9 0.4 convolution_convert_fusion
  94.8 0.8 pad_maximum_fusion.2.mixed_ref
  95.6 49.7 %shard_map.155 = bf16[4,4,64,256]{3,2,1,0:T(8,128)(2,1)} custom-call(bf16[2,128,1024]{2,1,0:T(8,128)(2,1)} %pad_maximum_fusion.2.mixed_ref, bf16[2,1024,256]{2,1,0:T(8,128)(2,1)} %rest_0_.1, bf16[2,1024,256]{2,1,0:T(8,128)(2,1)} %copy-done, bf16[2,1024,256]{2,1,0:T(8,128)(2,1)} %get-tuple-element.40.rest_2_), custom_call_target="tpu_custom_call" | custom-call | tf_op jit(solution)/shard_map/pallas_call | solution.py:427
  145.3 1.4 copy.155
  146.7 1.2 reshape.504
  (133 shorter events, 7.1 us)
Async XLA Ops:
  0.0 8.2 %copy-start.6 = (bf16[128,512]{1,0:T(8,128)(2,1)S(1)}, bf16[128,512]{1,0:T(8,128)(2,1)}, u32[]{:S(2)}) copy-start(bf16[128,512]{1,0:T(8,128)(2,1)} %param.22) | copy-start | bytes 393220
  0.0 8.3 %copy-start.7 = (bf16[128,512]{1,0:T(8,128)(2,1)S(1)}, bf16[128,512]{1,0:T(8,128)(2,1)}, u32[]{:S(2)}) copy-start(bf16[128,512]{1,0:T(8,128)(2,1)} %param.21) | copy-start | bytes 393220
  0.0 8.5 %copy-start.3 = (bf16[128,1024]{1,0:T(8,128)(2,1)S(1)}, bf16[128,1024]{1,0:T(8,128)(2,1)}, u32[]{:S(2)}) copy-start(bf16[128,1024]{1,0:T(8,128)(2,1)} %param.20) | copy-start | bytes 786436
  3.2 39.8 %collective-permute-start.1 = (bf16[128,1024]{0,1:T(8,128)(2,1)}, bf16[128,1024]{0,1:T(8,128)(2,1)}, u32[]{:S(2)}, u32[]{:S(2)}) collective-permute-start(bf16[128,1024]{0,1:T(8,128)(2,1)} %pad_maximum_fusion.3), channel_id=1, source_target_pairs={{2,0},{4,2},{6,4},{8,6},{10,8},{12,10},{14,12},{16,14},{18,16},{20... | collective-permute-start | bytes 786440 | tf_op jit(solution)/shard_map/ppermute | solution.py:32
  4.5 40.3 %collective-permute-start = (bf16[128,1024]{0,1:T(8,128)(2,1)}, bf16[128,1024]{0,1:T(8,128)(2,1)}, u32[]{:S(2)}, u32[]{:S(2)}) collective-permute-start(bf16[128,1024]{0,1:T(8,128)(2,1)} %pad_maximum_fusion.3), channel_id=1, source_target_pairs={{0,2},{2,4},{4,6},{6,8},{8,10},{10,12},{12,14},{14,16},{16,18},{18... | collective-permute-start | bytes 786440 | tf_op jit(solution)/shard_map/ppermute | solution.py:30
  8.7 10.6 %copy-start.37 = (f32[2,16]{1,0:T(2,128)S(1)}, f32[2,16]{1,0:T(2,128)}, u32[]{:S(2)}) copy-start(f32[2,16]{1,0:T(2,128)} %param.27) | copy-start | bytes 388
  8.7 10.6 %copy-start.21 = (f32[2,16,128]{2,1,0:T(8,128)S(1)}, f32[2,16,128]{2,1,0:T(8,128)}, u32[]{:S(2)}) copy-start(f32[2,16,128]{2,1,0:T(8,128)} %param.26) | copy-start | bytes 49156
  8.7 10.6 %copy-start.22 = (f32[2,16,128]{2,1,0:T(8,128)S(1)}, f32[2,16,128]{2,1,0:T(8,128)}, u32[]{:S(2)}) copy-start(f32[2,16,128]{2,1,0:T(8,128)} %param.28) | copy-start | bytes 49156
  9.9 14.3 %copy-start.19 = (bf16[5,1024]{1,0:T(8,128)(2,1)S(1)}, bf16[5,1024]{1,0:T(8,128)(2,1)}, u32[]{:S(2)}) copy-start(bf16[5,1024]{1,0:T(8,128)(2,1)} %param.23) | copy-start | bytes 30724
  9.9 14.3 %copy-start.28 = (bf16[5,512]{1,0:T(8,128)(2,1)S(1)}, bf16[5,512]{1,0:T(8,128)(2,1)}, u32[]{:S(2)}) copy-start(bf16[5,512]{1,0:T(8,128)(2,1)} %param.24) | copy-start | bytes 15364
  9.9 14.3 %copy-start.29 = (bf16[5,512]{1,0:T(8,128)(2,1)S(1)}, bf16[5,512]{1,0:T(8,128)(2,1)}, u32[]{:S(2)}) copy-start(bf16[5,512]{1,0:T(8,128)(2,1)} %param.25) | copy-start | bytes 15364
  9.9 23.5 %collective-permute-start.2 = (bf16[2,2048]{0,1:T(8,128)(2,1)}, bf16[2,2048]{0,1:T(8,128)(2,1)}, u32[]{:S(2)}, u32[]{:S(2)}) collective-permute-start(bf16[2,2048]{0,1:T(8,128)(2,1)} %get-tuple-element.49), channel_id=1, source_target_pairs={{0,2},{2,4},{4,6},{6,8},{8,10},{10,12},{12,14},{14,16},{16,18},{18... | collective-permute-start | bytes 24584 | tf_op jit(solution)/shard_map/ppermute | solution.py:30
  14.7 18.7 %collective-permute-start.3 = (bf16[2,2048]{0,1:T(8,128)(2,1)}, bf16[2,2048]{0,1:T(8,128)(2,1)}, u32[]{:S(2)}, u32[]{:S(2)}) collective-permute-start(bf16[2,2048]{0,1:T(8,128)(2,1)} %get-tuple-element.50), channel_id=1, source_target_pairs={{2,0},{4,2},{6,4},{8,6},{10,8},{12,10},{14,12},{16,14},{18,16},{20... | collective-permute-start | bytes 24584 | tf_op jit(solution)/shard_map/ppermute | solution.py:32
  16.0 33.9 %collective-permute-start.4 = (bf16[2,1024,256]{2,1,0:T(8,128)(2,1)}, bf16[2,1024,256]{2,1,0:T(8,128)(2,1)S(1)}, u32[]{:S(2)}, u32[]{:S(2)}) collective-permute-start(bf16[2,1024,256]{2,1,0:T(8,128)(2,1)} %rest_0_.1), channel_id=1, source_target_pairs={{0,8},{2,10},{4,12},{6,14},{8,16},{10,18},{12,20},{14,22},{16,24},... | collective-permute-start | bytes 3145736 | tf_op jit(solution)/shard_map/ppermute | solution.py:405
  19.4 5.6 %copy-start.4 = (bf16[128,1024]{1,0:T(8,128)(2,1)S(1)}, bf16[128,1024]{1,0:T(8,128)(2,1)}, u32[]{:S(2)}) copy-start(bf16[128,1024]{1,0:T(8,128)(2,1)} %param.16) | copy-start | bytes 786436
  25.2 2.6 %copy-start.27 = (s32[384]{0:T(512)S(1)}, s32[384]{0:T(512)}, u32[]{:S(2)}) copy-start(s32[384]{0:T(512)} %iota_add_fusion.1) | copy-start | bytes 4612
  29.6 11.5 %copy-start.30 = (f32[128,4,4]{0,2,1:T(4,128)}, f32[128,4,4]{0,2,1:T(4,128)S(1)}, u32[]{:S(2)}) copy-start(f32[128,4,4]{0,2,1:T(4,128)S(1)} %rev.20) | copy-start | bytes 24580
  33.3 1.9 %copy-start.12 = (f32[1,2048]{1,0:T(1,128)S(1)}, f32[1,2048]{1,0:T(1,128)}, u32[]{:S(2)}) copy-start(f32[1,2048]{1,0:T(1,128)} %get-tuple-element.69) | copy-start | bytes 24580
  33.3 1.9 %copy-start.13 = (f32[1,2048]{1,0:T(1,128)S(1)}, f32[1,2048]{1,0:T(1,128)}, u32[]{:S(2)}) copy-start(f32[1,2048]{1,0:T(1,128)} %get-tuple-element.70) | copy-start | bytes 24580
  33.3 1.9 %copy-start.14 = (f32[1,2048]{1,0:T(1,128)S(1)}, f32[1,2048]{1,0:T(1,128)}, u32[]{:S(2)}) copy-start(f32[1,2048]{1,0:T(1,128)} %get-tuple-element.71) | copy-start | bytes 24580
  33.3 1.9 %copy-start.15 = (f32[1,2048]{1,0:T(1,128)S(1)}, f32[1,2048]{1,0:T(1,128)}, u32[]{:S(2)}) copy-start(f32[1,2048]{1,0:T(1,128)} %get-tuple-element.72) | copy-start | bytes 24580
  33.4 1.9 %copy-start.16 = (f32[1,2048]{1,0:T(1,128)S(1)}, f32[1,2048]{1,0:T(1,128)}, u32[]{:S(2)}) copy-start(f32[1,2048]{1,0:T(1,128)} %get-tuple-element.73) | copy-start | bytes 24580
  39.8 1.3 copy-start.36
  39.8 1.8 %copy-start.32 = (f32[1,128,16]{1,2,0:T(8,128)S(1)}, f32[1,128,16]{1,2,0:T(8,128)}, u32[]{:S(2)}) copy-start(f32[1,128,16]{1,2,0:T(8,128)} %get-tuple-element.74) | copy-start | bytes 24580
  39.8 1.8 %copy-start.35 = (f32[4,4]{1,0:T(4,128)S(1)}, f32[4,4]{1,0:T(4,128)}, u32[]{:S(2)}) copy-start(f32[4,4]{1,0:T(4,128)} %get-tuple-element.65) | copy-start | bytes 196
  42.7 7.2 %copy-start.18 = (f32[4,2,4]{2,1,0:T(2,128)S(1)}, f32[4,2,4]{2,1,0:T(2,128)}, u32[]{:S(2)}) copy-start(f32[4,2,4]{2,1,0:T(2,128)} %copy.133) | copy-start | bytes 388
  43.0 45.1 %copy-start.24 = (f32[4,4]{1,0:T(4,128)S(1)}, f32[4,4]{1,0:T(4,128)}, u32[]{:S(2)}) copy-start(f32[4,4]{1,0:T(4,128)} %get-tuple-element.66) | copy-start | bytes 196
  44.7 44.5 %copy-start.20 = (pred[128,128]{1,0:T(8,128)(4,1)S(1)}, pred[128,128]{1,0:T(8,128)(4,1)}, u32[]{:S(2)}) copy-start(pred[128,128]{1,0:T(8,128)(4,1)} %iota_compare_fusion) | copy-start | bytes 49156
  44.8 44.5 %copy-start.26 = (f32[128,4,4]{0,2,1:T(4,128)S(1)}, f32[128,4,4]{0,2,1:T(4,128)}, u32[]{:S(2)}) copy-start(f32[128,4,4]{0,2,1:T(4,128)} %copy.140) | copy-start | bytes 24580
  44.8 44.5 %copy-start.33 = (f32[1,128,16]{1,2,0:T(8,128)S(1)}, f32[1,128,16]{1,2,0:T(8,128)}, u32[]{:S(2)}) copy-start(f32[1,128,16]{1,2,0:T(8,128)} %get-tuple-element.74) | copy-start | bytes 24580
  49.8 1.0 copy-start
  89.3 1.0 copy-start.2
  89.3 1.0 copy-start.23
  89.3 1.3 copy-start.25
  89.3 1.3 copy-start.31
  90.7 1.0 copy-start.1
  91.9 1.0 copy-start.5
  91.9 1.0 copy-start.8
  91.9 1.0 copy-start.11
  92.7 0.7 copy-start.17
  92.9 1.0 copy-start.9
  92.9 1.0 copy-start.10
  93.8 0.7 copy-start.34
